TPU v7x, 32 devices: a whole 2x2x4 slice. The times are simulated.
32 devices in a mesh: sp: 16 (over z, y, core), tp: 2 (over x).
Axes of the slice: x: 2, y: 2, z: 4, core: 2. Of those that a mesh axis runs over, the one named last changes fastest.
Arguments:
- layer_source_rows: bfloat16 [6144, 2048], P(('sp', 'tp')), may hold values from -6 to 6
- entry_rescale_factor: bfloat16 [2048], replicated, may hold values from 0.099609375 to 1.8984375
- sliding_mixer_entry_matrix: bfloat16 [3, 2048, 1024], P(None, 'sp', 'tp'), may hold values from -0.125 to 0.125
- recurrent_mixer_entry_matrix: bfloat16 [2, 2048, 1024], P(None, 'sp', 'tp'), may hold values from -0.125 to 0.125
- latent_write_read_matrix: bfloat16 [2, 2048, 2048], P(None, 'sp', 'tp'), may hold values from -0.125 to 0.125
- timestep_matrix: bfloat16 [2048, 2, 16], P(None, None, 'tp'), may hold values from -0.125 to 0.125
- sliding_kernel_coefficients: bfloat16 [3, 1024], P(None, 'tp'), may hold values from -3.5 to 3.5
- recurrent_kernel_coefficients: bfloat16 [5, 1024], P(None, 'tp'), may hold values from -0.5 to 0.5
- latent_kernel_coefficients: bfloat16 [5, 2, 2048], P(None, None, 'tp'), may hold values from -0.5 to 0.5
- lane_forgetting_rate: float32 [2, 16], P(None, 'tp'), may hold values from 0 to 1
- spike_forgetting_rate: float32 [6144, 16], P('sp', 'tp'), may hold values from -2 to 0
- lane_rescale_factor: bfloat16 [1024], P('tp'), may hold values from 0.099609375 to 1.8984375
- sliding_mixer_exit_matrix: bfloat16 [1024, 2048], P('tp', 'sp'), may hold values from -0.125 to 0.125
- recurrent_mixer_exit_matrix: bfloat16 [1024, 2048], P('tp', 'sp'), may hold values from -0.125 to 0.125
Outputs:
- mixed_out: bfloat16 [6144, 2048], P(('sp', 'tp'))
All inputs are finite; a program needn't handle non-finite values.
Results may differ from a plain program's by a relative error of at most 0.017.
Values may be sent and summed in bfloat16 or wider, within the bound.
A program may use at most 64 MiB of HBM per device.

v0:
```python
import jax
import jax.numpy as jnp
from jax import lax
from jax.sharding import PartitionSpec as P

HEAD_DIM = 64
STATE = 128
BLOCK = 128


epsilon = 1e-05


def carried_in(value, axis, join, neutral):
    count, mine = (lax.axis_size(axis), lax.axis_index(axis))
    pieces = jax.tree.map(lambda part: lax.all_gather(part, axis), value)
    pieces = jax.tree.map(lambda part: part[::-1], pieces)
    mine = count - 1 - mine
    subtotal = jax.tree.map(
        lambda part, zero: jnp.full_like(part, 0) + jnp.asarray(zero, part.dtype), value, neutral
    )

    def lap(position, subtotal):
        longer = join(subtotal, jax.tree.map(lambda part: part[position], pieces))
        return jax.tree.map(lambda new, old: jnp.where(position < mine, new, old), longer, subtotal)

    return lax.fori_loop(0, count - 1, lap, subtotal)


def entering_2(value, axis, join, neutral):
    place = lax.axis_index(axis)
    gathered = jax.tree.map(
        lambda a, kind: lax.all_gather(a.astype(kind), axis), value, (jnp.bfloat16, jnp.bfloat16)
    )
    state = jax.tree.map(lambda a, e: jnp.zeros_like(a) + jnp.asarray(e, a.dtype), value, neutral)

    def one(lap, state):
        return join(
            state,
            jax.tree.map(
                lambda a, own: lax.dynamic_index_in_dim(a, lap, 0, False).astype(own.dtype),
                gathered,
                value,
            ),
        )

    return lax.fori_loop(0, place, one, state)


def padded_2(value, sides, width):
    for axis, dim in sides:
        size, length = (lax.axis_size(axis), value.shape[dim])
        up = [(i, (i + 1) % size) for i in range(size - 1)]
        down = [(j, i) for i, j in up]
        last = lax.slice_in_dim(value, length - width, length, axis=dim)
        leading = lax.slice_in_dim(value, 0, width, axis=dim)
        before = lax.ppermute(last, axis, up)
        after = lax.ppermute(leading, axis, down)
        value = jnp.concatenate([before, value, after], axis=dim)
    return value


def apply_taps(padded, tap_table, length):
    summed = jnp.zeros((length, padded.shape[1]), jnp.float32)
    for offset in range(tap_table.shape[0]):
        summed = summed + padded[offset : offset + length].astype(jnp.float32) * tap_table[
            offset
        ].astype(jnp.float32)
    return summed


def local_blocks(ssd_x, keys_b, reads_c, timestep_deltas, forgetting_exponent):
    length, groups, per_group, head_dim = ssd_x.shape
    blocks = length // BLOCK
    x_blocks = ssd_x.reshape(blocks, BLOCK, groups, per_group, head_dim)
    b_blocks = keys_b.reshape(blocks, BLOCK, groups, STATE)
    c_blocks = reads_c.reshape(blocks, BLOCK, groups, STATE)
    d_blocks = timestep_deltas.reshape(blocks, BLOCK, groups, per_group)
    l_blocks = forgetting_exponent.reshape(blocks, BLOCK, groups, per_group)
    lower_mask = (jnp.arange(BLOCK)[:, None] >= jnp.arange(BLOCK)[None, :])[None, :, :, None, None]
    running = jnp.cumsum(l_blocks, axis=1)
    log_gaps = jnp.where(lower_mask, running[:, :, None] - running[:, None, :], 0.0)
    decays = jnp.where(lower_mask, jnp.exp(log_gaps), 0.0)
    scores = jnp.einsum("btgn,bsgn->btsg", c_blocks, b_blocks, preferred_element_type=jnp.float32)
    weights = (scores[..., None] * decays * d_blocks[:, None]).astype(jnp.bfloat16)
    within = jnp.einsum("btsgr,bsgrp->btgrp", weights, x_blocks, preferred_element_type=jnp.float32)
    to_end = jnp.exp(running[:, -1:] - running) * d_blocks
    weighted = (x_blocks.astype(jnp.float32) * to_end[..., None]).astype(jnp.bfloat16)
    contribution = jnp.einsum(
        "bsgrp,bsgn->bgrpn", weighted, b_blocks, preferred_element_type=jnp.float32
    )
    return (within, contribution, running, c_blocks)


def combine(earlier, following):
    return (earlier[0] * following[0], earlier[1] * following[0][..., None, None] + following[1])


def run_direction(ssd_x, keys_b, reads_c, timestep_deltas, forgetting_exponent, backward):
    within, contribution, running, c_blocks = local_blocks(
        ssd_x, keys_b, reads_c, timestep_deltas, forgetting_exponent
    )
    block_ends = running[:, -1]

    def chain_step(carry_state, inputs):
        part_state, block_end = inputs
        return (carry_state * jnp.exp(block_end)[..., None, None] + part_state, carry_state)

    summed, before = lax.scan(
        chain_step, jnp.zeros_like(contribution[0]), (contribution, block_ends)
    )
    device_decay = jnp.exp(jnp.sum(block_ends, axis=0))
    identity = (jnp.ones_like(device_decay), jnp.zeros_like(summed))
    if backward:
        incoming = carried_in((device_decay, summed), "sp", combine, identity)
    else:
        incoming = entering_2((device_decay, summed), "sp", combine, identity)
    starts = jnp.cumsum(block_ends, axis=0) - block_ends
    entering = (before + incoming[1][None] * jnp.exp(starts)[..., None, None]).astype(jnp.bfloat16)
    carried = jnp.einsum(
        "btgn,bgrpn->btgrp", c_blocks, entering, preferred_element_type=jnp.float32
    )
    carried = carried * jnp.exp(running)[..., None]
    return (within + carried).reshape(ssd_x.shape)


def local(
    layer_source_rows,
    entry_rescale_factor,
    sliding_mixer_entry_matrix,
    recurrent_mixer_entry_matrix,
    latent_write_read_matrix,
    timestep_matrix,
    sliding_kernel_coefficients,
    recurrent_kernel_coefficients,
    latent_kernel_coefficients,
    lane_forgetting_rate,
    spike_forgetting_rate,
    lane_rescale_factor,
    sliding_mixer_exit_matrix,
    recurrent_mixer_exit_matrix,
):
    float_rows = layer_source_rows.astype(jnp.float32)
    normed = (
        float_rows
        * lax.rsqrt(jnp.mean(float_rows * float_rows, axis=-1, keepdims=True) + epsilon)
        * entry_rescale_factor.astype(jnp.float32)
    ).astype(jnp.bfloat16)
    (
        sliding_mixer_entry_matrix,
        recurrent_mixer_entry_matrix,
        latent_write_read_matrix,
        sliding_mixer_exit_matrix,
        recurrent_mixer_exit_matrix,
    ) = (
        lax.all_gather(sliding_mixer_entry_matrix, "sp", axis=1, tiled=True),
        lax.all_gather(recurrent_mixer_entry_matrix, "sp", axis=1, tiled=True),
        lax.all_gather(latent_write_read_matrix, "sp", axis=1, tiled=True),
        lax.all_gather(sliding_mixer_exit_matrix, "sp", axis=1, tiled=True),
        lax.all_gather(recurrent_mixer_exit_matrix, "sp", axis=1, tiled=True),
    )
    conv_width = sliding_mixer_entry_matrix.shape[2]
    ssd_width = recurrent_mixer_entry_matrix.shape[2]
    state_width = latent_write_read_matrix.shape[2]
    local_heads = timestep_matrix.shape[2]
    step_weight = timestep_matrix.reshape(timestep_matrix.shape[0], 2 * local_heads)
    row_piece = lax.all_gather(normed, "tp", axis=0, tiled=True)
    row_count = row_piece.shape[0]
    conv_cols = jnp.einsum(
        "rd,kdc->rkc", row_piece, sliding_mixer_entry_matrix, preferred_element_type=jnp.float32
    ).reshape(row_count, -1)
    ssd_cols = jnp.einsum(
        "rd,kdc->rkc", row_piece, recurrent_mixer_entry_matrix, preferred_element_type=jnp.float32
    ).reshape(row_count, -1)
    state_cols = jnp.einsum(
        "rd,kdc->rkc", row_piece, latent_write_read_matrix, preferred_element_type=jnp.float32
    ).reshape(row_count, -1)
    step_cols = jnp.dot(row_piece, step_weight, preferred_element_type=jnp.float32)
    projected = jnp.concatenate([conv_cols, ssd_cols, state_cols, step_cols], axis=1).astype(
        jnp.bfloat16
    )
    length = projected.shape[0]
    out_gate = projected[:, :conv_width]
    in_gate = projected[:, conv_width : 2 * conv_width]
    values = projected[:, 2 * conv_width : 3 * conv_width]
    gate_start = 3 * conv_width
    ssd_gate = projected[:, gate_start : gate_start + ssd_width]
    joined = projected[:, gate_start + ssd_width : gate_start + 2 * ssd_width + 2 * state_width]
    raw_step = projected[:, gate_start + 2 * ssd_width + 2 * state_width :].reshape(
        length, 2, local_heads
    )
    gated_in = (in_gate.astype(jnp.float32) * values.astype(jnp.float32)).astype(jnp.bfloat16)
    gated_pad = padded_2(gated_in, (("sp", 0),), 1)
    joined_pad = padded_2(joined, (("sp", 0),), 2)
    y_conv = (
        out_gate.astype(jnp.float32) * apply_taps(gated_pad, sliding_kernel_coefficients, length)
    ).astype(jnp.bfloat16)
    joined_taps = jnp.concatenate(
        [
            recurrent_kernel_coefficients,
            latent_kernel_coefficients.reshape(latent_kernel_coefficients.shape[0], -1),
        ],
        axis=1,
    )
    mixed_ssd = jax.nn.silu(apply_taps(joined_pad, joined_taps, length)).astype(jnp.bfloat16)
    local_groups = state_width // STATE
    per_group = local_heads // local_groups
    ssd_x = mixed_ssd[:, :ssd_width].reshape(length, local_groups, per_group, HEAD_DIM)
    keys_b = mixed_ssd[:, ssd_width : ssd_width + state_width].reshape(length, local_groups, STATE)
    reads_c = mixed_ssd[:, ssd_width + state_width :].reshape(length, local_groups, STATE)
    timestep_deltas = jax.nn.softplus(raw_step.astype(jnp.float32))
    forgetting_exponent = (
        -timestep_deltas * lane_forgetting_rate[None] + spike_forgetting_rate[:, None, :]
    )
    head_shape = (length, local_groups, per_group)
    y_fwd = run_direction(
        ssd_x,
        keys_b,
        reads_c,
        timestep_deltas[:, 0].reshape(head_shape),
        forgetting_exponent[:, 0].reshape(head_shape),
        False,
    )
    y_bwd = jnp.flip(
        run_direction(
            jnp.flip(ssd_x, 0),
            jnp.flip(keys_b, 0),
            jnp.flip(reads_c, 0),
            jnp.flip(timestep_deltas[:, 1].reshape(head_shape), 0),
            jnp.flip(forgetting_exponent[:, 1].reshape(head_shape), 0),
            True,
        ),
        0,
    )
    gated_out = (y_fwd + y_bwd).reshape(length, ssd_width) * jax.nn.silu(
        ssd_gate.astype(jnp.float32)
    )
    grouped = gated_out.reshape(length, local_groups, per_group * HEAD_DIM)
    grouped = grouped * lax.rsqrt(jnp.mean(grouped * grouped, axis=-1, keepdims=True) + epsilon)
    y_ssd = (grouped.reshape(length, ssd_width) * lane_rescale_factor.astype(jnp.float32)).astype(
        jnp.bfloat16
    )
    return lax.psum_scatter(
        (
            jnp.dot(y_conv, sliding_mixer_exit_matrix, preferred_element_type=jnp.float32)
            + jnp.dot(y_ssd, recurrent_mixer_exit_matrix, preferred_element_type=jnp.float32)
        ).astype(jnp.bfloat16),
        "tp",
        scatter_dimension=0,
        tiled=True,
    )


def solution(mesh):
    placed = (
        P(("sp", "tp"), None),
        P(),
        P(None, "sp", "tp"),
        P(None, "sp", "tp"),
        P(None, "sp", "tp"),
        P(None, None, "tp"),
        P(None, "tp"),
        P(None, "tp"),
        P(None, None, "tp"),
        P(None, "tp"),
        P("sp", "tp"),
        P("tp"),
        P("tp", "sp"),
        P("tp", "sp"),
    )
    return jax.shard_map(
        local, mesh=mesh, in_specs=placed, out_specs=P(("sp", "tp"), None), check_vma=False
    )
```

profile of v0, /device:TPU:0, one launch (start us, length us, event | category | flops | bytes accessed | tf_op | source)
XLA Modules:
  0.0 444.4 jit_solution(14916279932055997721)
XLA Ops:
  8.7 2.3 fusion.12
  14.5 26.6 %all-gather.13.cloned.1.call-done = bf16[384,2048]{1,0:T(8,128)(2,1)} async-done(((bf16[192,2048]{1,0:T(8,128)(2,1)}), bf16[384,2048]{1,0:T(8,128)(2,1)}) %all-gather.13.cloned.1.call-update) | async-done | bytes 1572880 | tf_op jit(solution)/shard_map/all_gather | solution.py:167
  43.6 71.1 %fusion.94 = f32[3,128,8,1]{3,2,1,0:T(8,128)S(1)} fusion(f32[3,128,8,1]{3,2,1,0:T(8,128)S(1)} %copy.85), kind=kOutput, calls=%fused_computation.163 | output fusion | flops 390144 | bytes 24576 | tf_op jit(solution)/shard_map/jit(cumsum)/reduce_window_sum | solution.py:81
  115.5 4.6 %fusion.25 = bf16[384,2,512]{2,0,1:T(8,128)(2,1)S(1)} fusion(bf16[2,2048,512]{2,1,0:T(8,128)(2,1)} %all-gather.19.cloned.1.call-done, bf16[384,2048]{1,0:T(8,128)(2,1)} %all-gather.13.cloned.1.call-done), kind=kOutput, calls=%fused_computation.50 | convolution fusion | flops 1611005952 | bytes 6553600 | tf_op jit(solution)/shard_map/rd,kdc->rkc/dot_general | solution.py:172
  120.5 48.3 %all-gather.21.cloned.1.call-done = bf16[2,2048,1024]{2,1,0:T(8,128)(2,1)} async-done(((bf16[2,128,1024]{2,1,0:T(8,128)(2,1)}), bf16[2,2048,1024]{2,1,0:T(8,128)(2,1)}) %all-gather.21.cloned.1.call-update) | async-done | bytes 8388624 | tf_op jit(solution)/shard_map/all_gather | solution.py:158
  168.7 7.9 %convolution_convert_fusion = bf16[384,2,1024]{2,0,1:T(8,128)(2,1)} fusion(bf16[2,2048,1024]{2,1,0:T(8,128)(2,1)} %all-gather.21.cloned.1.call-done, bf16[384,2048]{1,0:T(8,128)(2,1)S(1)} %copy-done.14), kind=kOutput, calls=%fused_computation.34 | convolution fusion | flops 3222011904 | bytes 11534336 | tf_op jit(solution)/shard_map/rd,kdc->rkc/dot_general | solution.py:175
  187.3 11.5 %multiply_convert_fusion = bf16[384,2560]{0,1:T(8,128)(2,1)S(1)} fusion(bf16[384,2560]{0,1:T(8,128)(2,1)} %fusion.7, bf16[2,2560]{0,1:T(8,128)(2,1)S(1)} %copy.80, bf16[2,2560]{0,1:T(8,128)(2,1)S(1)} %copy.78, f32[2560]{0:T(1024)S(1)} %get-tuple-element.354, f32[2560]{0:T(1024)S(1)} %get-tuple-element.355, f32[2560]{0:T(1024)S(1)} %copy-done.16, ...), kind=kLoop, calls=%fused_computation.19 | loop fusion | flops 30474240 | bytes 4003840 | tf_op jit(solution)/shard_map/convert_element_type | solution.py:205
  215.4 15.4 %all-gather.15.cloned.1.call-done = bf16[3,2048,512]{2,1,0:T(8,128)(2,1)} async-done(((bf16[3,128,512]{2,1,0:T(8,128)(2,1)}), bf16[3,2048,512]{2,1,0:T(8,128)(2,1)}) %all-gather.15.cloned.1.call-update) | async-done | bytes 6291472 | tf_op jit(solution)/shard_map/all_gather | solution.py:156
  230.9 6.4 %fusion.22 = bf16[384,3,512]{2,0,1:T(8,128)(2,1)} fusion(bf16[3,2048,512]{2,1,0:T(8,128)(2,1)} %all-gather.15.cloned.1.call-done, bf16[384,2048]{1,0:T(8,128)(2,1)S(1)} %copy-done.15), kind=kOutput, calls=%fused_computation.49 | convolution fusion | flops 2416508928 | bytes 9043968 | tf_op jit(solution)/shard_map/rd,kdc->rkc/dot_general | solution.py:169
  243.9 32.6 %all-reduce = bf16[128]{0:T(256)(128)(2,1)S(1)} all-reduce(bf16[128]{0:T(256)(128)(2,1)S(1)} %dynamic-update-slice), channel_id=2, replica_groups=mesh['sp'=16,'tp'=2] {'sp'}, use_global_device_ids=true, to_apply=%add | all-reduce | flops 128 | bytes 512
  276.6 30.0 %all-reduce.1 = f32[128]{0:T(128)S(1)} all-reduce(f32[128]{0:T(128)S(1)} %exponential_dynamic-update-slice_fusion), channel_id=4, replica_groups=mesh['sp'=16,'tp'=2] {'sp'}, use_global_device_ids=true, to_apply=%add.1 | all-reduce | flops 128 | bytes 1024
  306.7 3.6 fusion.62
  310.3 3.3 reshape.401
  315.9 2.4 copy.98
  320.5 3.6 fusion.37
  324.1 3.7 fusion.36
  328.0 3.2 fusion.32
  331.2 35.6 %all-gather.27.cloned.1.call-done = f32[128,1,64,128]{3,2,1,0:T(8,128)} async-done(((f32[8,1,64,128]{3,2,1,0:T(8,128)}), f32[128,1,64,128]{3,2,1,0:T(8,128)}) %all-gather.27.cloned.1.call-update) | async-done | bytes 4194320 | tf_op jit(solution)/shard_map/all_gather | solution.py:16
  366.8 4.8 %rev.34 = f32[16,8,1,64,128]{4,3,1,2,0:T(8,128)} reverse(f32[16,8,1,64,128]{4,3,1,2,0:T(8,128)} %bitcast.263), dimensions={0} | reverse | bytes 8388608 | tf_op jit(solution)/shard_map/rev | solution.py:17
  371.6 16.4 %while.55 = (s32[]{:T(128)}, f32[8,1,64,128]{3,2,1,0:T(8,128)S(1)}, s32[]{:T(128)}, f32[16,8,1]{1,2,0:T(1,128)S(1)}, f32[16,8,1,64,128]{4,3,1,2,0:T(8,128)}, /*index=5*/s32[]{:T(128)}, s32[]{:T(128)}) while((s32[]{:T(128)}, f32[8,1,64,128]{3,2,1,0:T(8,128)S(1)}, s32[]{:T(128)}, f32[16,8,1]{1,2,0:T(1,128)S(1)}, ...), condition=%wide.region_13.14_spmd.clone, body=%wide.region_12.13_spmd.clone.sunk | while | flops 262148 | bytes 786633 | solution.py:27
  391.2 3.0 rev.35
  397.2 11.3 %all-gather.23.cloned.1.call-done = bf16[512,2048]{1,0:T(8,128)(2,1)} async-done(((bf16[512,128]{1,0:T(8,128)(2,1)}), bf16[512,2048]{1,0:T(8,128)(2,1)}) %all-gather.23.cloned.1.call-update) | async-done | bytes 2097168 | tf_op jit(solution)/shard_map/all_gather | solution.py:160
  408.6 3.9 add_convert_fusion
  412.5 25.4 %reduce-scatter.2.cloned.1.call-done = bf16[192,2048]{1,0:T(8,128)(2,1)} async-done(((bf16[384,2048]{1,0:T(8,128)(2,1)}), bf16[192,2048]{1,0:T(8,128)(2,1)}) %reduce-scatter.2.cloned.1.call-update) | async-done | bytes 786448 | tf_op jit(solution)/shard_map/reduce_scatter | solution.py:243
  (210 shorter events, 69.7 us)
Async XLA Ops:
  6.5 34.5 %copy-start = (bf16[2048,2,8]{0,2,1:T(8,128)(2,1)S(1)}, bf16[2048,2,8]{0,2,1:T(8,128)(2,1)}, u32[]{:S(2)}) copy-start(bf16[2048,2,8]{0,2,1:T(8,128)(2,1)} %param.27) | copy-start | bytes 196612
  6.5 34.5 %all-gather.13.cloned.1.call-start = ((), (), s32[]{:S(2)}) async-start(), calls=%async_computation.1 | async-start | bytes 2359296 | tf_op jit(solution)/shard_map/all_gather | solution.py:167
  8.6 5.1 %copy-start.21 = (bf16[5,512]{1,0:T(8,128)(2,1)S(1)}, bf16[5,512]{1,0:T(8,128)(2,1)}, u32[]{:S(2)}) copy-start(bf16[5,512]{1,0:T(8,128)(2,1)} %param.29) | copy-start | bytes 15364
  8.6 5.1 %copy-start.18 = (bf16[5,2,1024]{2,1,0:T(2,128)(2,1)S(1)}, bf16[5,2,1024]{2,1,0:T(2,128)(2,1)}, u32[]{:S(2)}) copy-start(bf16[5,2,1024]{2,1,0:T(2,128)(2,1)} %param.30) | copy-start | bytes 61444
  8.7 32.4 %copy-start.19 = (f32[384,8]{0,1:T(8,128)S(1)}, f32[384,8]{0,1:T(8,128)}, u32[]{:S(2)}) copy-start(f32[384,8]{0,1:T(8,128)} %param.32) | copy-start | bytes 36868
  8.7 32.4 %copy-start.23 = (f32[2,8]{1,0:T(2,128)S(1)}, f32[2,8]{1,0:T(2,128)}, u32[]{:S(2)}) copy-start(f32[2,8]{1,0:T(2,128)} %param.31) | copy-start | bytes 196
  11.0 104.5 %all-gather.19.cloned.1.call-start = ((), (), s32[]{:S(2)}) async-start(), calls=%async_computation.4 | async-start | bytes 4456448 | tf_op jit(solution)/shard_map/all_gather | solution.py:157
  11.8 157.0 %all-gather.21.cloned.1.call-start = ((), (), s32[]{:S(2)}) async-start(), calls=%async_computation.5 | async-start | bytes 8912896 | tf_op jit(solution)/shard_map/all_gather | solution.py:158
  12.5 218.4 %all-gather.15.cloned.1.call-start = ((), (), s32[]{:S(2)}) async-start(), calls=%async_computation.2 | async-start | bytes 6684672 | tf_op jit(solution)/shard_map/all_gather | solution.py:156
  13.1 293.6 %all-gather.17.cloned.1.call-start = ((), (), s32[]{:S(2)}) async-start(), calls=%async_computation.3 | async-start | bytes 2228224 | tf_op jit(solution)/shard_map/all_gather | solution.py:159
  13.6 314.1 %all-gather.25.cloned.1.call-start = ((), (), s32[]{:S(2)}) async-start(), calls=%async_computation.8 | async-start | bytes 2228224 | tf_op jit(solution)/shard_map/all_gather | solution.py:33
  115.5 53.3 %copy-start.14 = (bf16[384,2048]{1,0:T(8,128)(2,1)S(1)}, bf16[384,2048]{1,0:T(8,128)(2,1)}, u32[]{:S(2)}) copy-start(bf16[384,2048]{1,0:T(8,128)(2,1)} %all-gather.13.cloned.1.call-done) | copy-start | bytes 4718596
  120.5 64.5 %copy-start.3 = (bf16[384,2,512]{0,2,1:T(8,128)(2,1)}, bf16[384,2,512]{0,2,1:T(8,128)(2,1)S(1)}, u32[]{:S(2)}) copy-start(bf16[384,2,512]{0,2,1:T(8,128)(2,1)S(1)} %copy.75) | copy-start | bytes 2359300
  181.1 5.3 %collective-permute-start.2 = (bf16[2,2560]{1,0:T(2,128)(2,1)S(1)}, bf16[2,2560]{1,0:T(2,128)(2,1)S(1)}, u32[]{:S(2)}, u32[]{:S(2)}) collective-permute-start(bf16[2,2560]{1,0:T(2,128)(2,1)S(1)} %copy.77), channel_id=1, source_target_pairs={{0,2},{2,4},{4,6},{6,8},{8,10},{10,12},{12,14},{14,16},{16,18},{18... | collective-permute-start | bytes 30728 | tf_op jit(solution)/shard_map/ppermute | solution.py:57
  183.5 3.3 collective-permute-start.3
  204.6 162.2 %all-gather.27.cloned.1.call-start = ((), (), s32[]{:S(2)}) async-start(), calls=%async_computation.9 | async-start | bytes 4456448 | tf_op jit(solution)/shard_map/all_gather | solution.py:16
  211.8 19.0 %copy-start.15 = (bf16[384,2048]{1,0:T(8,128)(2,1)S(1)}, bf16[384,2048]{1,0:T(8,128)(2,1)}, u32[]{:S(2)}) copy-start(bf16[384,2048]{1,0:T(8,128)(2,1)} %all-gather.13.cloned.1.call-done) | copy-start | bytes 4718596
  212.3 18.5 %copy-start.10 = (f32[3,8,1,64,128]{4,3,1,2,0:T(8,128)}, f32[3,8,1,64,128]{4,3,1,2,0:T(8,128)S(1)}, u32[]{:S(2)}) copy-start(f32[3,8,1,64,128]{4,3,1,2,0:T(8,128)S(1)} %get-tuple-element.202) | copy-start | bytes 2359300
  213.1 195.5 %all-gather.23.cloned.1.call-start = ((), (), s32[]{:S(2)}) async-start(), calls=%async_computation.6 | async-start | bytes 2228224 | tf_op jit(solution)/shard_map/all_gather | solution.py:160
  213.8 224.1 %reduce-scatter.2.cloned.1.call-start = ((), (), s32[]{:S(2)}) async-start(), calls=%async_computation.7 | async-start | bytes 2359296 | tf_op jit(solution)/shard_map/reduce_scatter | solution.py:243
  239.0 67.7 %copy-start.6 = (bf16[384,3,512]{0,2,1:T(8,128)(2,1)}, bf16[384,3,512]{0,2,1:T(8,128)(2,1)S(1)}, u32[]{:S(2)}) copy-start(bf16[384,3,512]{0,2,1:T(8,128)(2,1)S(1)} %copy.74) | copy-start | bytes 3538948
  240.1 66.6 %collective-permute-start = (bf16[1,512]{0,1:T(8,128)(2,1)S(1)}, bf16[1,512]{0,1:T(8,128)(2,1)S(1)}, u32[]{:S(2)}, u32[]{:S(2)}) collective-permute-start(bf16[1,512]{0,1:T(8,128)(2,1)S(1)} %get-tuple-element.402), channel_id=1, source_target_pairs={{0,2},{2,4},{4,6},{6,8},{8,10},{10,12},{12,14},{14,16},{16,18},{18... | collective-permute-start | bytes 3080 | tf_op jit(solution)/shard_map/ppermute | solution.py:57
  242.3 64.4 %collective-permute-start.1 = (bf16[1,512]{0,1:T(8,128)(2,1)S(1)}, bf16[1,512]{0,1:T(8,128)(2,1)S(1)}, u32[]{:S(2)}, u32[]{:S(2)}) collective-permute-start(bf16[1,512]{0,1:T(8,128)(2,1)S(1)} %get-tuple-element.403), channel_id=1, source_target_pairs={{2,0},{4,2},{6,4},{8,6},{10,8},{12,10},{14,12},{16,14},{18,16},{20... | collective-permute-start | bytes 3080 | tf_op jit(solution)/shard_map/ppermute | solution.py:58
  408.6 29.3 %copy-start.1 = (bf16[2048,2,8]{0,2,1:T(8,128)(2,1)S(1)}, bf16[2048,2,8]{0,2,1:T(8,128)(2,1)}, u32[]{:S(2)}) copy-start(bf16[2048,2,8]{0,2,1:T(8,128)(2,1)} %param.27) | copy-start | bytes 196612
  (14 other events, 28.1 us)
Sparse Core Ops, SparseCore 0:
  11.1 29.8 all-gather.12
  43.2 50.3 all-gather.18
  95.9 72.8 all-gather.20
  170.8 60.0 all-gather.14
  232.8 39.8 all-gather.16
  274.8 40.6 all-gather.24
  317.6 49.1 all-gather.26
  368.9 39.5 all-gather.22
  412.6 25.2 reduce-scatter.1
where the time goes:
time: 446 us; the launch traced here: 444 us
  waiting for transfers between devices  166 us (37%)
  other arithmetic  113 us (25%)
  blocking collectives  62.5 us (14%)
  matrix products  41.8 us (9%)
  local copies, waits for them, and re-layouts  38.1 us (9%)
  between operations  14.6 us (3%)
  starting transfers between devices  7.53 us (2%)
    another operation x2, other arithmetic, local_blocks(): running = jnp.cumsum(l_blocks, axis=1)  72.7 us
    unnamed x2, blocking collectives  62.5 us
    all_gather x1, waiting for transfers between devices, local(): lax.all_gather(latent_write_read_matrix, 'sp', axis=1, tiled=True)  48.3 us
    all_gather x1, waiting for transfers between devices, carried_in(): pieces = jax.tree.map(lambda part: lax.all_gather(part, axis), value)  35.6 us
    all_gather x1, waiting for transfers between devices, local(): row_piece = lax.all_gather(normed, 'tp', axis=0, tiled=True)  26.6 us
    reduce_scatter x1, waiting for transfers between devices, local(): lax.psum_scatter((jnp.dot(y_conv, sliding_mixer_exit_matrix, preferred_el...  25.4 us
    select_n x15, other arithmetic, lap(): jnp.where(position < mine, new, old)  15.8 us
    all_gather x1, waiting for transfers between devices, local(): lax.all_gather(sliding_mixer_entry_matrix, 'sp', axis=1, tiled=True)  15.4 us
  transfers between devices with their start and end apart: 13, of which 6 were waited for; matrix products, arithmetic and copies ran while one was open for 41% of the time, Pallas kernels for 0%

commit v1 on v0

v1 whole, which is shorter than its diff:
```python
import functools

import jax
import jax.numpy as jnp
from jax import lax
from jax.experimental import pallas as pl
from jax.experimental.pallas import tpu as pltpu
from jax.sharding import PartitionSpec as P

HEAD_DIM = 64
STATE = 128
HALO = 8
CHUNKS = 2
epsilon = 1e-05
F32 = jnp.float32
BF16 = jnp.bfloat16
HIGHEST = lax.Precision.HIGHEST


def ring_kernel(n, w_ref, out_ref, own_sem, ring_send, ring_recv, mate_send, mate_recv):
    chips = n // 2
    me = lax.axis_index("sp")
    core, chip = me % 2, me // 2
    odd = chip % 2
    spot = (1 - odd) * (chip // 2) + odd * (chips - 1 - chip // 2)

    def device(position):
        position = (position + 2 * chips) % chips
        half = (chips + 1) // 2
        late = position // half
        late_chip = 2 * (chips - 1 - position) + 1
        return 2 * ((1 - late) * 2 * position + late * late_chip) + core

    mate = me + 1 - 2 * core
    ways = (device(spot + 1), device(spot - 1))
    rows = w_ref.shape[0] // (2 * CHUNKS)

    barrier = pltpu.get_barrier_semaphore()
    for other in (mate,) + ways:
        pl.semaphore_signal(
            barrier, inc=1, device_id={"sp": other}, device_id_type=pl.DeviceIdType.MESH
        )
    pl.semaphore_wait(barrier, 3)

    def piece(way, chunk):
        return pl.ds((way * CHUNKS + chunk) * rows, rows)

    def ring_copy(step, way, chunk):
        owner = device(spot - step if way == 0 else spot + step)
        part = piece(way, chunk)
        return pltpu.make_async_remote_copy(
            src_ref=w_ref.at[part] if step == 0 else out_ref.at[owner, part],
            dst_ref=out_ref.at[owner, part],
            send_sem=ring_send.at[step, way, chunk],
            recv_sem=ring_recv.at[step, way, chunk],
            device_id={"sp": ways[way]},
            device_id_type=pl.DeviceIdType.MESH,
        )

    def arrival(step, way, chunk):
        owner = device(spot - step - 1 if way == 0 else spot + step + 1)
        part = piece(way, chunk)
        return pltpu.make_async_remote_copy(
            src_ref=out_ref.at[owner, part],
            dst_ref=out_ref.at[owner, part],
            send_sem=ring_send.at[step, way, chunk],
            recv_sem=ring_recv.at[step, way, chunk],
            device_id={"sp": ways[way]},
            device_id_type=pl.DeviceIdType.MESH,
        )

    def mate_copy(step, way, chunk, incoming=False):
        owner = device(spot - step if way == 0 else spot + step)
        if incoming:
            owner = owner + 1 - 2 * core
        part = piece(way, chunk)
        return pltpu.make_async_remote_copy(
            src_ref=w_ref.at[part] if step == 0 else out_ref.at[owner, part],
            dst_ref=out_ref.at[owner, part],
            send_sem=mate_send.at[step, way, chunk],
            recv_sem=mate_recv.at[step, way, chunk],
            device_id={"sp": mate},
            device_id_type=pl.DeviceIdType.MESH,
        )

    parts = [(way, chunk) for chunk in range(CHUNKS) for way in range(2)]
    for way, chunk in parts:
        ring_copy(0, way, chunk).start()
    for way, chunk in parts:
        mate_copy(0, way, chunk).start()
    own = pltpu.make_async_copy(w_ref, out_ref.at[me], own_sem)
    own.start()
    for step in range(chips - 1):
        for way, chunk in parts:
            arrival(step, way, chunk).wait_recv()
            if step < chips - 2:
                ring_copy(step + 1, way, chunk).start()
            mate_copy(step + 1, way, chunk).start()
    own.wait()
    for step in range(chips):
        for way, chunk in parts:
            if step < chips - 1:
                ring_copy(step, way, chunk).wait_send()
            mate_copy(step, way, chunk).wait_send()
            mate_copy(step, way, chunk, True).wait_recv()


def gather_rows(block):
    n = lax.axis_size("sp")
    chips = n // 2
    rows, cols = block.shape
    return pl.pallas_call(
        functools.partial(ring_kernel, n),
        out_shape=jax.ShapeDtypeStruct((n, rows, cols), block.dtype),
        in_specs=[pl.BlockSpec(memory_space=pltpu.VMEM)],
        out_specs=pl.BlockSpec(memory_space=pl.ANY),
        scratch_shapes=[
            pltpu.SemaphoreType.DMA,
            pltpu.SemaphoreType.DMA((chips - 1, 2, CHUNKS)),
            pltpu.SemaphoreType.DMA((chips - 1, 2, CHUNKS)),
            pltpu.SemaphoreType.DMA((chips, 2, CHUNKS)),
            pltpu.SemaphoreType.DMA((chips, 2, CHUNKS)),
        ],
        compiler_params=pltpu.CompilerParams(
            collective_id=0, has_side_effects=True, vmem_limit_bytes=16 * 2**20
        ),
        cost_estimate=pl.CostEstimate(
            flops=0, bytes_accessed=n * rows * cols * 16, transcendentals=0
        ),
    )(block)


def taps_of(padded, table, length):
    full = padded.shape[0]
    half = table.shape[0] // 2
    total = None
    for k in range(table.shape[0]):
        moved = padded if k == half else pltpu.roll(padded, (half - k) % full, 0)
        term = moved[HALO : HALO + length] * table[k : k + 1].astype(F32)
        total = term if total is None else total + term
    return total


def silu(v):
    return v * jax.nn.sigmoid(v)


def mix_kernel(
    og_ref, ig_ref, va_ref, x_ref, b_ref, c_ref, ct_ref, xt_ref, bt_ref, rt_ref,
    col_ref, row_ref, yconv_ref, within_ref, reads_ref, state_ref,
):
    length = yconv_ref.shape[0]
    gated = (ig_ref[...].astype(F32) * va_ref[...].astype(F32)).astype(BF16).astype(F32)
    conv = taps_of(gated, ct_ref[...], length)
    yconv_ref[...] = (og_ref[pl.ds(HALO, length), :].astype(F32) * conv).astype(BF16)
    xs = silu(taps_of(x_ref[...].astype(F32), xt_ref[...], length)).astype(BF16)
    bs = silu(taps_of(b_ref[...].astype(F32), bt_ref[...], length)).astype(BF16)
    cs = silu(taps_of(c_ref[...].astype(F32), rt_ref[...], length)).astype(BF16)
    reads_ref[...] = cs
    cols = col_ref[0]
    rows = row_ref[0]
    t_at = lax.broadcasted_iota(jnp.int32, (length, length), 0)
    s_at = lax.broadcasted_iota(jnp.int32, (length, length), 1)
    outs, weighted = [], []
    for h in range(2):
        c_h = cs[:, h * STATE : (h + 1) * STATE]
        b_h = bs[:, h * STATE : (h + 1) * STATE]
        x_h = xs[:, h * HEAD_DIM : (h + 1) * HEAD_DIM]
        o = 4 * h
        scores = lax.dot_general(
            c_h, b_h, (((1,), (1,)), ((), ())), preferred_element_type=F32
        )
        gap = jnp.where(
            t_at >= s_at,
            cols[:, o + 2 : o + 3] - rows[o + 2 : o + 3],
            cols[:, o + 3 : o + 4] - rows[o + 3 : o + 4],
        )
        d_f, d_b = rows[o : o + 1], rows[o + 1 : o + 2]
        scale = jnp.where(t_at > s_at, d_f, jnp.where(t_at < s_at, d_b, d_f + d_b))
        w = (scores * jnp.exp(gap) * scale).astype(BF16)
        outs.append(jnp.dot(w, x_h, preferred_element_type=F32))
        x32 = x_h.astype(F32)
        end_f = jnp.exp(rows[o + 2 : o + 3, length - 1 : length] - cols[:, o + 2 : o + 3])
        end_b = jnp.exp(rows[o + 3 : o + 4, 0:1] - cols[:, o + 3 : o + 4])
        both = jnp.concatenate(
            [x32 * (end_f * cols[:, o : o + 1]), x32 * (end_b * cols[:, o + 1 : o + 2])], axis=1
        ).astype(BF16)
        state_ref[h * STATE : (h + 1) * STATE] = lax.dot_general(
            both, b_h, (((0,), (0,)), ((), ())), preferred_element_type=F32
        ).astype(BF16)
    within_ref[...] = jnp.concatenate(outs, axis=1)


def chain_kernel(s_ref, d_ref, back_ref, out_ref):
    n = s_ref.shape[0]
    back = back_ref[...] > 0.5
    acc = jnp.zeros(s_ref.shape[1:], F32)
    fwd = []
    for j in range(n):
        fwd.append(acc)
        acc = acc * d_ref[j] + s_ref[j].astype(F32)
    acc = jnp.zeros(s_ref.shape[1:], F32)
    for j in reversed(range(n)):
        out_ref[j] = jnp.where(back, acc, fwd[j]).astype(BF16)
        acc = acc * d_ref[j] + s_ref[j].astype(F32)


def finish_kernel(within_ref, reads_ref, enter_ref, gate_ref, gain_ref, col_ref, y_ref):
    length = y_ref.shape[0]
    cols = col_ref[0]
    outs = []
    for h in range(2):
        o = 4 * h
        both = lax.dot_general(
            reads_ref[:, h * STATE : (h + 1) * STATE],
            enter_ref[h * STATE : (h + 1) * STATE],
            (((1,), (1,)), ((), ())),
            preferred_element_type=F32,
        )
        here = slice(h * HEAD_DIM, (h + 1) * HEAD_DIM)
        y = within_ref[:, here]
        y = y + both[:, :HEAD_DIM] * jnp.exp(cols[:, o + 2 : o + 3])
        y = y + both[:, HEAD_DIM:] * jnp.exp(cols[:, o + 3 : o + 4])
        g = y * silu(gate_ref[pl.ds(HALO, length), :].astype(F32)[:, here])
        g = g * lax.rsqrt(jnp.mean(g * g, axis=-1, keepdims=True) + epsilon)
        outs.append(g * gain_ref[:, here].astype(F32))
    y_ref[...] = jnp.concatenate(outs, axis=1).astype(BF16)


def local(
    layer_source_rows, entry_rescale_factor, sliding_mixer_entry_matrix,
    recurrent_mixer_entry_matrix, latent_write_read_matrix, timestep_matrix,
    sliding_kernel_coefficients, recurrent_kernel_coefficients, latent_kernel_coefficients,
    lane_forgetting_rate, spike_forgetting_rate, lane_rescale_factor,
    sliding_mixer_exit_matrix, recurrent_mixer_exit_matrix,
):
    n = lax.axis_size("sp")
    tp = lax.axis_size("tp")
    own_rows, width = layer_source_rows.shape
    length = own_rows * tp
    full = length + 2 * HALO
    conv_width = sliding_mixer_entry_matrix.shape[2]
    ssd_width = recurrent_mixer_entry_matrix.shape[2]
    state_width = latent_write_read_matrix.shape[2]
    heads = timestep_matrix.shape[2]
    pairs = heads // 2
    cw = conv_width // pairs

    block = jnp.concatenate(
        [sliding_mixer_entry_matrix[i] for i in range(3)]
        + [recurrent_mixer_entry_matrix[i] for i in range(2)]
        + [latent_write_read_matrix[i] for i in range(2)],
        axis=1,
    )
    gathered = gather_rows(block)
    weights = gathered.reshape(n * block.shape[0], block.shape[1])

    x32 = layer_source_rows.astype(F32)
    normed = (
        x32
        * lax.rsqrt(jnp.mean(x32 * x32, axis=-1, keepdims=True) + epsilon)
        * entry_rescale_factor.astype(F32)
    ).astype(BF16)
    up = [(i, i + 1) for i in range(n - 1)]
    down = [(i + 1, i) for i in range(n - 1)]
    before = lax.ppermute(normed[own_rows - HALO :], "sp", up)
    after = lax.ppermute(normed[:HALO], "sp", down)
    shared = lax.all_gather(jnp.concatenate([before, normed, after], axis=0), "tp", axis=0)
    rows = jnp.concatenate(
        [shared[tp - 1, :HALO]]
        + [shared[i, HALO : HALO + own_rows] for i in range(tp)]
        + [shared[0, HALO + own_rows :]],
        axis=0,
    )

    step_weight = timestep_matrix.reshape(width, 2 * heads)
    raw = jnp.dot(rows, step_weight, preferred_element_type=F32).astype(BF16)
    raw = raw[HALO : HALO + length].astype(F32).reshape(length, 2, heads)
    deltas = jax.nn.softplus(raw)
    logs = -deltas * lane_forgetting_rate[None] + spike_forgetting_rate[:, None, :]
    tri = (jnp.arange(length)[:, None] >= jnp.arange(length)[None, :]).astype(F32)
    run_f = jnp.dot(tri, logs[:, 0], precision=HIGHEST)
    run_b = jnp.dot(tri.T, logs[:, 1], precision=HIGHEST)
    table = jnp.stack([deltas[:, 0], deltas[:, 1], run_f, run_b], axis=2)
    col_table = table.reshape(length, pairs, 8).transpose(1, 0, 2)
    row_table = table.reshape(length, pairs, 8).transpose(1, 2, 0)
    span_log = jnp.stack([run_f[length - 1], run_b[0]], axis=1)
    span_decay = jnp.exp(lax.all_gather(span_log, "sp")).reshape(n, heads * 2)
    span_decay = jnp.repeat(span_decay, HEAD_DIM, axis=1)
    share = heads * 2 * HEAD_DIM // n
    mine = lax.axis_index("sp") * share
    chain_decay = lax.dynamic_slice_in_dim(span_decay, mine, share, axis=1)[:, :, None]
    chain_back = ((mine + jnp.arange(share)) // HEAD_DIM % 2).astype(F32)[:, None]

    rows, weights = lax.optimization_barrier((rows, weights))
    proj = jnp.dot(rows, weights, preferred_element_type=F32).astype(BF16)

    exit_c, exit_s, proj = lax.optimization_barrier(
        (sliding_mixer_exit_matrix, recurrent_mixer_exit_matrix, proj)
    )
    exit_c = lax.all_gather(exit_c, "sp", axis=1, tiled=True)
    exit_s = lax.all_gather(exit_s, "sp", axis=1, tiled=True)

    latent = latent_kernel_coefficients
    pw, sw = 2 * HEAD_DIM, 2 * STATE
    g0 = 3 * conv_width
    at_gate, at_x = g0 // pw, (g0 + ssd_width) // pw
    at_b = (g0 + 2 * ssd_width) // sw
    at_c = at_b + pairs
    y_conv, within, reads, states = pl.pallas_call(
        mix_kernel,
        grid=(pairs,),
        in_specs=[
            pl.BlockSpec((full, cw), lambda j: (0, j)),
            pl.BlockSpec((full, cw), lambda j: (0, pairs + j)),
            pl.BlockSpec((full, cw), lambda j: (0, 2 * pairs + j)),
            pl.BlockSpec((full, pw), lambda j: (0, at_x + j)),
            pl.BlockSpec((full, sw), lambda j: (0, at_b + j)),
            pl.BlockSpec((full, sw), lambda j: (0, at_c + j)),
            pl.BlockSpec((3, cw), lambda j: (0, j)),
            pl.BlockSpec((5, pw), lambda j: (0, j)),
            pl.BlockSpec((5, sw), lambda j: (0, j)),
            pl.BlockSpec((5, sw), lambda j: (0, pairs + j)),
            pl.BlockSpec((1, length, 8), lambda j: (j, 0, 0)),
            pl.BlockSpec((1, 8, length), lambda j: (j, 0, 0)),
        ],
        out_specs=[
            pl.BlockSpec((length, cw), lambda j: (0, j)),
            pl.BlockSpec((length, pw), lambda j: (0, j)),
            pl.BlockSpec((length, sw), lambda j: (0, j)),
            pl.BlockSpec((sw, STATE), lambda j: (j, 0)),
        ],
        out_shape=[
            jax.ShapeDtypeStruct((length, conv_width), BF16),
            jax.ShapeDtypeStruct((length, ssd_width), F32),
            jax.ShapeDtypeStruct((length, state_width), BF16),
            jax.ShapeDtypeStruct((pairs * sw, STATE), BF16),
        ],
        cost_estimate=pl.CostEstimate(
            flops=8 * length * length * heads * STATE, bytes_accessed=2**24, transcendentals=0
        ),
    )(
        proj, proj, proj, proj, proj, proj,
        sliding_kernel_coefficients, recurrent_kernel_coefficients,
        latent.reshape(latent.shape[0], -1), latent.reshape(latent.shape[0], -1),
        col_table, row_table,
    )

    pieces = lax.all_to_all(states.reshape(n, share, STATE), "sp", 0, 0)
    entering = pl.pallas_call(
        chain_kernel, out_shape=jax.ShapeDtypeStruct((n, share, STATE), BF16)
    )(pieces, chain_decay, chain_back)
    entering = lax.all_to_all(entering, "sp", 0, 0).reshape(pairs * sw, STATE)

    y_ssd = pl.pallas_call(
        finish_kernel,
        grid=(pairs,),
        in_specs=[
            pl.BlockSpec((length, pw), lambda j: (0, j)),
            pl.BlockSpec((length, sw), lambda j: (0, j)),
            pl.BlockSpec((sw, STATE), lambda j: (j, 0)),
            pl.BlockSpec((full, pw), lambda j: (0, at_gate + j)),
            pl.BlockSpec((1, pw), lambda j: (0, j)),
            pl.BlockSpec((1, length, 8), lambda j: (j, 0, 0)),
        ],
        out_specs=pl.BlockSpec((length, pw), lambda j: (0, j)),
        out_shape=jax.ShapeDtypeStruct((length, ssd_width), BF16),
    )(within, reads, entering, proj, lane_rescale_factor.reshape(1, -1), col_table)

    partial = (
        jnp.dot(y_conv, exit_c, preferred_element_type=F32)
        + jnp.dot(y_ssd, exit_s, preferred_element_type=F32)
    ).astype(BF16)
    return lax.psum_scatter(partial, "tp", scatter_dimension=0, tiled=True)


def solution(mesh):
    placed = (
        P(("sp", "tp"), None),
        P(),
        P(None, "sp", "tp"),
        P(None, "sp", "tp"),
        P(None, "sp", "tp"),
        P(None, None, "tp"),
        P(None, "tp"),
        P(None, "tp"),
        P(None, None, "tp"),
        P(None, "tp"),
        P("sp", "tp"),
        P("tp"),
        P("tp", "sp"),
        P("tp", "sp"),
    )
    return jax.shard_map(
        local, mesh=mesh, in_specs=placed, out_specs=P(("sp", "tp"), None), check_vma=False
    )
```

time: 446 us -> 261 us (0.59)
  Pallas kernels: 0 us -> 116 us
  waiting for transfers between devices: 166 us -> 54.7 us
  other arithmetic: 113 us -> 5.36 us
  blocking collectives: 62.5 us -> 21.8 us
  local copies, waits for them, and re-layouts: 38.1 us -> 14.4 us
  matrix products: 41.8 us -> 20.5 us
  starting transfers between devices: 7.53 us -> 13.5 us
    all_gather x8 -> x3, waiting for transfers between devices: 137 us -> 16.1 us  [the longest x1 16.1 us: local(): exit_s = lax.all_gather(exit_s, 'sp', axis=1, tiled=True)]
    pallas_call x0 -> x4, Pallas kernels: none -> 116 us  [the longest x1 99 us: gather_rows(): pl.pallas_call(functools.partial(ring_kernel, n), out_shape=jax.ShapeDtyp...]
    another operation x4 -> x1, other arithmetic: 72.8 us -> 0.03 us  [local(): table = jnp.stack([deltas[:, 0], deltas[:, 1], run_f, run_b], axis=2)]
    unnamed x2 -> x0, blocking collectives: 62.5 us -> none
    all_gather x0 -> x1, blocking collectives: none -> 21.8 us  [local(): span_decay = jnp.exp(lax.all_gather(span_log, 'sp')).reshape(n, heads * 2)]
    dot_general x12 -> x6, matrix products: 41.8 us -> 20.5 us  [the longest x1 12.9 us: local(): proj = jnp.dot(rows, weights, preferred_element_type=F32).astype(BF16)]
    select_n x15 -> x1, other arithmetic: 15.8 us -> 0.12 us  [local(): deltas = jax.nn.softplus(raw)]
    convert_element_type x10 -> x3, other arithmetic: 16.8 us -> 2.76 us  [the longest x1 1.38 us: local(): normed = (x32 * lax.rsqrt(jnp.mean(x32 * x32, axis=-1, keepdims=True) + e...]
  transfers between devices with their start and end apart: 13 -> 8, of which waited for: 6 -> 4; matrix products, arithmetic and copies ran while one was open for 41% -> 3% of each run, Pallas kernels for 0% -> 45%
where the time goes in v1:
time: 261 us; the launch traced here: 260 us
  Pallas kernels  116 us (44%)
  waiting for transfers between devices  54.7 us (21%)
  blocking collectives  21.8 us (8%)
  matrix products  20.5 us (8%)
  local copies, waits for them, and re-layouts  14.4 us (6%)
  starting transfers between devices  13.5 us (5%)
  between operations  13.4 us (5%)
  other arithmetic  5.36 us (2%)
    pallas_call x1, Pallas kernels, gather_rows(): pl.pallas_call(functools.partial(ring_kernel, n), out_shape=jax.ShapeDtyp...  99 us
    reduce_scatter x1, waiting for transfers between devices, local(): return lax.psum_scatter(partial, 'tp', scatter_dimension=0, tiled=True)  25.4 us
    all_gather x1, blocking collectives, local(): span_decay = jnp.exp(lax.all_gather(span_log, 'sp')).reshape(n, heads * 2)  21.8 us
    all_gather x1, waiting for transfers between devices, local(): exit_s = lax.all_gather(exit_s, 'sp', axis=1, tiled=True)  16.1 us
    dot_general x1, matrix products, local(): proj = jnp.dot(rows, weights, preferred_element_type=F32).astype(BF16)  12.9 us
    all_to_all x1, waiting for transfers between devices, local(): entering = lax.all_to_all(entering, 'sp', 0, 0).reshape(pairs * sw, STATE)  11.6 us
    pallas_call x1, Pallas kernels, local(): pl.pallas_call(mix_kernel, grid=(pairs,), in_specs=[pl.BlockSpec((full, c...  10.2 us
    unnamed x31, local copies, waits for them, and re-layouts  8.59 us
  transfers between devices with their start and end apart: 8, of which 4 were waited for; matrix products, arithmetic and copies ran while one was open for 3% of the time, Pallas kernels for 45%

profile of v1, /device:TPU:0, one launch (start us, length us, event | category | flops | bytes accessed | tf_op | source)
XLA Modules:
  0.0 260.3 jit_solution(15838230633312850537)
XLA Ops:
  7.3 1.4 fusion
  8.6 1.4 fusion.2
  10.1 1.4 collective-permute-start.1
  11.5 3.2 %collective-permute-start = (bf16[8,2048]{1,0:T(8,128)(2,1)S(1)}, bf16[8,2048]{1,0:T(8,128)(2,1)S(1)}, u32[]{:S(2)}, u32[]{:S(2)}) collective-permute-start(bf16[8,2048]{1,0:T(8,128)(2,1)S(1)} %get-tuple-element.27), channel_id=1, source_target_pairs={{0,2},{2,4},{4,6},{6,8},{8,10},{10,12},{12,14},{14,16},{16,18},{18... | collective-permute-start | bytes 98312 | tf_op jit(solution)/shard_map/ppermute | solution.py:266
  14.7 0.8 collective-permute-done
  15.5 1.0 pad_maximum_fusion.1
  16.7 99.0 %shard_map.136 = bf16[16,128,4608]{2,1,0:T(8,128)(2,1)S(1)} custom-call(bf16[128,4608]{1,0:T(8,128)(2,1)S(1)} %bitcast_dynamic-update-slice_fusion.w_ref), custom_call_target="tpu_custom_call" | custom-call | bytes 150994944 | tf_op jit(solution)/shard_map/pallas_call | solution.py:112
  115.7 6.4 %copy-done.1 = bf16[16,128,4608]{2,1,0:T(8,128)(2,1)} copy-done((bf16[16,128,4608]{2,1,0:T(8,128)(2,1)}, bf16[16,128,4608]{2,1,0:T(8,128)(2,1)S(1)}, u32[]{:S(2)}) %copy-start.1) | copy-done | bytes 18874392
  122.2 0.8 slice_bitcast_fusion.3
  122.9 1.5 slice_bitcast_fusion.1
  124.5 12.9 %convolution_convert_fusion.og_ref.ig_ref.va_ref.x_ref.b_ref.c_ref.gate_ref = bf16[400,4608]{1,0:T(8,128)(2,1)} fusion(bf16[400,2048]{1,0:T(8,128)(2,1)S(1)} %pad_maximum_fusion, bf16[2048,4608]{1,0:T(8,128)(2,1)} %bitcast.68), kind=kOutput, calls=%fused_computation | convolution fusion | flops 7551590400 | bytes 24199168 | tf_op jit(solution)/shard_map/dot_general | solution.py:296
  140.1 1.2 copy.27
  141.3 10.2 %shard_map.137 = (bf16[384,512]{1,0:T(8,128)(2,1)}, f32[384,512]{1,0:T(8,128)}, bf16[384,1024]{1,0:T(8,128)(2,1)}, bf16[1024,128]{1,0:T(8,128)(2,1)}) custom-call(bf16[400,4608]{1,0:T(8,128)(2,1)} %convolution_convert_fusion.og_ref.ig_ref.va_ref.x_ref.b_ref.c_ref.gate_ref, ...), custom_call_target="tpu_custom_call" | custom-call | flops 1207959552 | bytes 16777216 | tf_op jit(solution)/shard_map/pallas_call | solution.py:310
  151.5 5.3 %all-to-all-start = ((bf16[16,64,128]{2,1,0:T(8,128)(2,1)}), bf16[16,64,128]{2,1,0:T(8,128)(2,1)S(1)}, u32[]{:S(2)}, u32[]{:S(2)}) async-start(bf16[16,64,128]{2,1,0:T(8,128)(2,1)} %bitcast.77), calls=%async_computation | async-start | bytes 524288 | tf_op jit(solution)/shard_map/all_to_all | solution.py:349
  157.8 21.8 %all-gather.2 = f32[16,8,2]{1,2,0:T(2,128)S(1)} all-gather(f32[1,8,2]{1,2,0:T(2,128)S(1)} %maximum_bitcast_fusion), channel_id=3, replica_groups=mesh['sp'=16,'tp'=2] {'sp'}, dimensions={0}, use_global_device_ids=true | all-gather | bytes 1088 | tf_op jit(solution)/shard_map/all_gather | solution.py:288
  180.0 1.1 copy.31.d_ref
  181.8 2.2 shard_map.138
  184.0 3.5 %all-to-all-start.1 = ((bf16[16,64,128]{2,1,0:T(8,128)(2,1)}), bf16[16,64,128]{2,1,0:T(8,128)(2,1)S(1)}, u32[]{:S(2)}, u32[]{:S(2)}) async-start(bf16[16,64,128]{2,1,0:T(8,128)(2,1)} %shard_map.138), calls=%async_computation.1 | async-start | bytes 524288 | tf_op jit(solution)/shard_map/all_to_all | solution.py:353
  188.1 11.6 %all-to-all-done.1 = bf16[16,64,128]{2,1,0:T(8,128)(2,1)S(1)} async-done(((bf16[16,64,128]{2,1,0:T(8,128)(2,1)}), bf16[16,64,128]{2,1,0:T(8,128)(2,1)S(1)}, u32[]{:S(2)}, u32[]{:S(2)}) %all-to-all-start.1) | async-done | bytes 262176 | tf_op jit(solution)/shard_map/all_to_all | solution.py:353
  200.5 5.2 %shard_map.139 = bf16[384,512]{1,0:T(8,128)(2,1)} custom-call(f32[384,512]{1,0:T(8,128)} %get-tuple-element.19.within_ref, bf16[384,1024]{1,0:T(8,128)(2,1)} %get-tuple-element.20.reads_ref, bf16[1024,128]{1,0:T(8,128)(2,1)} %bitcast.73, bf16[400,4608]{1,0:T(8,128)(2,1)} %convolution_convert_fusion.og_ref.ig_ref.va_ref.x_ref.b_ref.c_ref.gate_ref, ...), custom_call_target="tpu_custom_call" | custom-call | tf_op jit(solution)/shard_map/pallas_call | solution.py:355
  205.7 2.7 %fusion.18 = f32[384,2048]{1,0:T(8,128)S(1)} fusion(bf16[384,512]{1,0:T(8,128)(2,1)} %get-tuple-element.17, bf16[512,2048]{1,0:T(8,128)(2,1)} %all-gather.7.cloned.1.call-done), kind=kOutput, calls=%fused_computation.60 | convolution fusion | flops 805306368 | bytes 5636096 | tf_op jit(solution)/shard_map/dot_general | solution.py:371
  208.4 16.1 %all-gather.9.cloned.1.call-done = bf16[512,2048]{1,0:T(8,128)(2,1)} async-done(((bf16[512,128]{1,0:T(8,128)(2,1)}), bf16[512,2048]{1,0:T(8,128)(2,1)}) %all-gather.9.cloned.1.call-update) | async-done | bytes 2097168 | tf_op jit(solution)/shard_map/all_gather | solution.py:302
  224.5 3.9 %add_convert_fusion = bf16[384,2048]{1,0:T(8,128)(2,1)} fusion(f32[384,2048]{1,0:T(8,128)S(1)} %fusion.18, bf16[384,512]{1,0:T(8,128)(2,1)} %shard_map.139, bf16[512,2048]{1,0:T(8,128)(2,1)} %all-gather.9.cloned.1.call-done), kind=kOutput, calls=%fused_computation.1 | convolution fusion | flops 806879232 | bytes 7208960 | tf_op jit(solution)/shard_map/dot_general | solution.py:372
  228.4 25.4 %reduce-scatter.2.cloned.1.call-done = bf16[192,2048]{1,0:T(8,128)(2,1)} async-done(((bf16[384,2048]{1,0:T(8,128)(2,1)}), bf16[192,2048]{1,0:T(8,128)(2,1)}) %reduce-scatter.2.cloned.1.call-update) | async-done | bytes 786448 | tf_op jit(solution)/shard_map/reduce_scatter | solution.py:374
  (67 shorter events, 7.1 us)
Async XLA Ops:
  6.5 132.3 %copy-start = (bf16[2048,2,8]{0,2,1:T(8,128)(2,1)S(1)}, bf16[2048,2,8]{0,2,1:T(8,128)(2,1)}, u32[]{:S(2)}) copy-start(bf16[2048,2,8]{0,2,1:T(8,128)(2,1)} %param.19) | copy-start | bytes 196612
  6.5 115.6 %all-gather.11.cloned.1.call-start = ((), (), s32[]{:S(2)}) async-start(), calls=%async_computation.6 | async-start | bytes 2555904 | tf_op jit(solution)/shard_map/all_gather | solution.py:268
  10.0 6.5 %copy-start.6 = (bf16[3,128,512]{2,1,0:T(8,128)(2,1)S(1)}, bf16[3,128,512]{2,1,0:T(8,128)(2,1)}, u32[]{:S(2)}) copy-start(bf16[3,128,512]{2,1,0:T(8,128)(2,1)} %param.16) | copy-start | bytes 1179652
  10.1 4.6 %collective-permute-start.1 = (bf16[8,2048]{1,0:T(8,128)(2,1)S(1)}, bf16[8,2048]{1,0:T(8,128)(2,1)S(1)}, u32[]{:S(2)}, u32[]{:S(2)}) collective-permute-start(bf16[8,2048]{1,0:T(8,128)(2,1)S(1)} %get-tuple-element.28), channel_id=1, source_target_pairs={{2,0},{4,2},{6,4},{8,6},{10,8},{12,10},{14,12},{16,14},{18,16},{20... | collective-permute-start | bytes 98312 | tf_op jit(solution)/shard_map/ppermute | solution.py:267
  11.5 5.1 %copy-start.7 = (bf16[2,128,512]{2,1,0:T(8,128)(2,1)S(1)}, bf16[2,128,512]{2,1,0:T(8,128)(2,1)}, u32[]{:S(2)}) copy-start(bf16[2,128,512]{2,1,0:T(8,128)(2,1)} %param.17) | copy-start | bytes 786436
  11.5 5.2 %copy-start.4 = (bf16[2,128,1024]{2,1,0:T(8,128)(2,1)S(1)}, bf16[2,128,1024]{2,1,0:T(8,128)(2,1)}, u32[]{:S(2)}) copy-start(bf16[2,128,1024]{2,1,0:T(8,128)(2,1)} %param.18) | copy-start | bytes 1572868
  11.5 4.0 %collective-permute-start = (bf16[8,2048]{1,0:T(8,128)(2,1)S(1)}, bf16[8,2048]{1,0:T(8,128)(2,1)S(1)}, u32[]{:S(2)}, u32[]{:S(2)}) collective-permute-start(bf16[8,2048]{1,0:T(8,128)(2,1)S(1)} %get-tuple-element.27), channel_id=1, source_target_pairs={{0,2},{2,4},{4,6},{6,8},{8,10},{10,12},{12,14},{14,16},{16,18},{18... | collective-permute-start | bytes 98312 | tf_op jit(solution)/shard_map/ppermute | solution.py:266
  16.5 189.2 %all-gather.7.cloned.1.call-start = ((), (), s32[]{:S(2)}) async-start(), calls=%async_computation.3 | async-start | bytes 2228224 | tf_op jit(solution)/shard_map/all_gather | solution.py:301
  115.7 6.5 %copy-start.1 = (bf16[16,128,4608]{2,1,0:T(8,128)(2,1)}, bf16[16,128,4608]{2,1,0:T(8,128)(2,1)S(1)}, u32[]{:S(2)}) copy-start(bf16[16,128,4608]{2,1,0:T(8,128)(2,1)S(1)} %shard_map.136) | copy-start | bytes 56623108
  124.5 13.7 %copy-start.8 = (bf16[5,2,1024]{2,1,0:T(2,128)(2,1)S(1)}, bf16[5,2,1024]{2,1,0:T(2,128)(2,1)}, u32[]{:S(2)}) copy-start(bf16[5,2,1024]{2,1,0:T(2,128)(2,1)} %param.22) | copy-start | bytes 61444
  137.4 1.9 copy-start.9
  137.5 1.9 copy-start.10
  137.5 87.0 %all-gather.9.cloned.1.call-start = ((), (), s32[]{:S(2)}) async-start(), calls=%async_computation.4 | async-start | bytes 2228224 | tf_op jit(solution)/shard_map/all_gather | solution.py:302
  140.1 1.2 copy-start.5
  151.5 36.1 %copy-start.11 = (bf16[512]{0:T(512)(128)(2,1)S(1)}, bf16[512]{0:T(512)(128)(2,1)}, u32[]{:S(2)}) copy-start(bf16[512]{0:T(512)(128)(2,1)} %param.25) | copy-start | bytes 3076
  151.5 29.6 %all-to-all-start = ((bf16[16,64,128]{2,1,0:T(8,128)(2,1)}), bf16[16,64,128]{2,1,0:T(8,128)(2,1)S(1)}, u32[]{:S(2)}, u32[]{:S(2)}) async-start(bf16[16,64,128]{2,1,0:T(8,128)(2,1)} %bitcast.77), calls=%async_computation | async-start | bytes 524288 | tf_op jit(solution)/shard_map/all_to_all | solution.py:349
  181.1 0.7 copy-start.3
  184.0 15.8 %all-to-all-start.1 = ((bf16[16,64,128]{2,1,0:T(8,128)(2,1)}), bf16[16,64,128]{2,1,0:T(8,128)(2,1)S(1)}, u32[]{:S(2)}, u32[]{:S(2)}) async-start(bf16[16,64,128]{2,1,0:T(8,128)(2,1)} %shard_map.138), calls=%async_computation.1 | async-start | bytes 524288 | tf_op jit(solution)/shard_map/all_to_all | solution.py:353
  187.5 66.3 %reduce-scatter.2.cloned.1.call-start = ((), (), s32[]{:S(2)}) async-start(), calls=%async_computation.5 | async-start | bytes 2359296 | tf_op jit(solution)/shard_map/reduce_scatter | solution.py:374
  199.8 0.7 copy-start.2
Sparse Core Ops, SparseCore 0:
  16.6 34.1 all-gather.10
  137.6 41.9 all-gather.6
  181.8 42.7 all-gather.8
  228.5 25.2 reduce-scatter.1

commit v2 on v1

--- a/solution.py
+++ b/solution.py
@@ -191,18 +191,101 @@
     within_ref[...] = jnp.concatenate(outs, axis=1)
 
 
-def chain_kernel(s_ref, d_ref, back_ref, out_ref):
-    n = s_ref.shape[0]
-    back = back_ref[...] > 0.5
+def exchange_kernel(
+    n, share, s_ref, l_ref, out_ref, got, logs, enter, s_out, s_in, l_out, l_in, e_out, e_in
+):
+    me = lax.axis_index("sp")
+    barrier = pltpu.get_barrier_semaphore()
+    for k in range(1, n):
+        pl.semaphore_signal(
+            barrier,
+            inc=1,
+            device_id={"sp": (me + k) % n},
+            device_id_type=pl.DeviceIdType.MESH,
+        )
+    pl.semaphore_wait(barrier, n - 1)
+
+    def copy(src, dst, out_sem, in_sem, k, there, slot):
+        return pltpu.make_async_remote_copy(
+            src_ref=src.at[there],
+            dst_ref=dst.at[slot],
+            send_sem=out_sem.at[k],
+            recv_sem=in_sem.at[k],
+            device_id={"sp": there},
+            device_id_type=pl.DeviceIdType.MESH,
+        )
+
+    for k in range(1, n):
+        there = (me + k) % n
+        copy(s_ref, got, s_out, s_in, k, there, me).start()
+        copy(l_ref, logs, l_out, l_in, k, there, me).start()
+    got[me] = s_ref[me]
+    logs[me] = l_ref[me]
+    for k in range(1, n):
+        here = (me + n - k) % n
+        copy(s_ref, got, s_out, s_in, k, here, here).wait_recv()
+        copy(l_ref, logs, l_out, l_in, k, here, here).wait_recv()
+    back = (me * share // HEAD_DIM) % 2
     acc = jnp.zeros(s_ref.shape[1:], F32)
-    fwd = []
-    for j in range(n):
-        fwd.append(acc)
-        acc = acc * d_ref[j] + s_ref[j].astype(F32)
-    acc = jnp.zeros(s_ref.shape[1:], F32)
-    for j in reversed(range(n)):
-        out_ref[j] = jnp.where(back, acc, fwd[j]).astype(BF16)
-        acc = acc * d_ref[j] + s_ref[j].astype(F32)
+    for i in range(n):
+        j = back * (n - 1 - i) + (1 - back) * i
+        enter[j] = acc.astype(BF16)
+        acc = acc * jnp.exp(logs[j][0:1, :]) + got[j].astype(F32)
+    out_ref[me] = enter[me]
+    for k in range(1, n):
+        copy(enter, out_ref, e_out, e_in, k, (me + k) % n, me).start()
+    for k in range(1, n):
+        here = (me + n - k) % n
+        copy(enter, out_ref, e_out, e_in, k, here, here).wait_recv()
+    for k in range(1, n):
+        there = (me + k) % n
+        copy(s_ref, got, s_out, s_in, k, there, me).wait_send()
+        copy(l_ref, logs, l_out, l_in, k, there, me).wait_send()
+        copy(enter, out_ref, e_out, e_in, k, there, me).wait_send()
+
+
+def exchange_states(states, span_log):
+    n, share, _ = states.shape
+    assert HEAD_DIM % share == 0
+    tables = jnp.repeat(span_log.reshape(-1), HEAD_DIM // share)
+    tables = jnp.broadcast_to(tables[:, None, None], (n, 8, STATE))
+    return pl.pallas_call(
+        functools.partial(exchange_kernel, n, share),
+        out_shape=jax.ShapeDtypeStruct(states.shape, BF16),
+        in_specs=[pl.BlockSpec(memory_space=pltpu.VMEM)] * 2,
+        out_specs=pl.BlockSpec(memory_space=pltpu.VMEM),
+        scratch_shapes=[
+            pltpu.VMEM(states.shape, BF16),
+            pltpu.VMEM(tables.shape, F32),
+            pltpu.VMEM(states.shape, BF16),
+        ]
+        + [pltpu.SemaphoreType.DMA((n,))] * 6,
+        compiler_params=pltpu.CompilerParams(collective_id=1, has_side_effects=True),
+        cost_estimate=pl.CostEstimate(flops=0, bytes_accessed=2**25, transcendentals=0),
+    )(states, tables)
+
+
+def project_kernel(r_ref, w_ref, o_ref):
+    o_ref[...] = jnp.dot(r_ref[...], w_ref[...], preferred_element_type=F32).astype(BF16)
+
+
+def project(rows, weights):
+    count, width = rows.shape
+    cols = weights.shape[1]
+    tile = cols // 9
+    return pl.pallas_call(
+        project_kernel,
+        grid=(9,),
+        in_specs=[
+            pl.BlockSpec((count, width), lambda j: (0, 0)),
+            pl.BlockSpec((width, tile), lambda j: (0, j)),
+        ],
+        out_specs=pl.BlockSpec((count, tile), lambda j: (0, j)),
+        out_shape=jax.ShapeDtypeStruct((count, cols), BF16),
+        cost_estimate=pl.CostEstimate(
+            flops=2 * count * width * cols, bytes_accessed=2 * width * cols, transcendentals=0
+        ),
+    )(rows, weights)
 
 
 def finish_kernel(within_ref, reads_ref, enter_ref, gate_ref, gain_ref, col_ref, y_ref):
@@ -285,19 +368,12 @@
     col_table = table.reshape(length, pairs, 8).transpose(1, 0, 2)
     row_table = table.reshape(length, pairs, 8).transpose(1, 2, 0)
     span_log = jnp.stack([run_f[length - 1], run_b[0]], axis=1)
-    span_decay = jnp.exp(lax.all_gather(span_log, "sp")).reshape(n, heads * 2)
-    span_decay = jnp.repeat(span_decay, HEAD_DIM, axis=1)
     share = heads * 2 * HEAD_DIM // n
-    mine = lax.axis_index("sp") * share
-    chain_decay = lax.dynamic_slice_in_dim(span_decay, mine, share, axis=1)[:, :, None]
-    chain_back = ((mine + jnp.arange(share)) // HEAD_DIM % 2).astype(F32)[:, None]
-
-    rows, weights = lax.optimization_barrier((rows, weights))
-    proj = jnp.dot(rows, weights, preferred_element_type=F32).astype(BF16)
-
-    exit_c, exit_s, proj = lax.optimization_barrier(
-        (sliding_mixer_exit_matrix, recurrent_mixer_exit_matrix, proj)
-    )
+
+    exit_c, exit_s, weights = lax.optimization_barrier(
+        (sliding_mixer_exit_matrix, recurrent_mixer_exit_matrix, weights)
+    )
+    proj = project(rows, weights)
     exit_c = lax.all_gather(exit_c, "sp", axis=1, tiled=True)
     exit_s = lax.all_gather(exit_s, "sp", axis=1, tiled=True)
 
@@ -346,11 +422,8 @@
         col_table, row_table,
     )
 
-    pieces = lax.all_to_all(states.reshape(n, share, STATE), "sp", 0, 0)
-    entering = pl.pallas_call(
-        chain_kernel, out_shape=jax.ShapeDtypeStruct((n, share, STATE), BF16)
-    )(pieces, chain_decay, chain_back)
-    entering = lax.all_to_all(entering, "sp", 0, 0).reshape(pairs * sw, STATE)
+    entering = exchange_states(states.reshape(n, share, STATE), span_log)
+    entering = entering.reshape(pairs * sw, STATE)
 
     y_ssd = pl.pallas_call(
         finish_kernel,
@@ -367,11 +440,25 @@
         out_shape=jax.ShapeDtypeStruct((length, ssd_width), BF16),
     )(within, reads, entering, proj, lane_rescale_factor.reshape(1, -1), col_table)
 
-    partial = (
-        jnp.dot(y_conv, exit_c, preferred_element_type=F32)
-        + jnp.dot(y_ssd, exit_s, preferred_element_type=F32)
-    ).astype(BF16)
-    return lax.psum_scatter(partial, "tp", scatter_dimension=0, tiled=True)
+    def partial(y_c, y_s):
+        return (
+            jnp.dot(y_c, exit_c, preferred_element_type=F32)
+            + jnp.dot(y_s, exit_s, preferred_element_type=F32)
+        ).astype(BF16)
+
+    if tp != 2:
+        return lax.psum_scatter(
+            partial(y_conv, y_ssd), "tp", scatter_dimension=0, tiled=True
+        )
+    tp_me = lax.axis_index("tp")
+
+    def rows_of(owner, y):
+        return lax.dynamic_slice_in_dim(y, owner * own_rows, own_rows, axis=0)
+
+    away = partial(rows_of(1 - tp_me, y_conv), rows_of(1 - tp_me, y_ssd))
+    arrived = lax.ppermute(away, "tp", [(0, 1), (1, 0)])
+    kept = partial(rows_of(tp_me, y_conv), rows_of(tp_me, y_ssd))
+    return (kept.astype(F32) + arrived.astype(F32)).astype(BF16)
 
 
 def solution(mesh):

time: 261 us -> 240 us (0.920)
  Pallas kernels: 116 us -> 147 us
  blocking collectives: 21.8 us -> 0 us
  waiting for transfers between devices: 54.7 us -> 43.5 us
  matrix products: 20.5 us -> 11.4 us
  starting transfers between devices: 13.5 us -> 5.69 us
    pallas_call x1 -> x2, Pallas kernels: 2.15 us -> 34.3 us  [the longest x1 19.1 us: exchange_states(): pl.pallas_call(functools.partial(exchange_kernel, n, share), out_shape=ja...]
    reduce_scatter x1 -> x0, waiting for transfers between devices: 25.4 us -> none  [local(): return lax.psum_scatter(partial, 'tp', scatter_dimension=0, tiled=True)]
    all_gather x1 -> x0, blocking collectives: 21.8 us -> none  [local(): span_decay = jnp.exp(lax.all_gather(span_log, 'sp')).reshape(n, heads * 2)]
    ppermute x0 -> x1, waiting for transfers between devices: none -> 16.5 us  [local(): arrived = lax.ppermute(away, 'tp', [(0, 1), (1, 0)])]
    all_to_all x2 -> x0, waiting for transfers between devices: 11.6 us -> none  [the longest x1 11.6 us: local(): entering = lax.all_to_all(entering, 'sp', 0, 0).reshape(pairs * sw, STATE)]
    dot_general x3 -> x4, matrix products: 19.5 us -> 10.3 us  [the longest x2 5.27 us: partial(): jnp.dot(y_s, exit_s, preferred_element_type=F32)]
    all_to_all x2 -> x0, starting transfers between devices: 8.83 us -> none  [the longest x1 5.3 us: local(): pieces = lax.all_to_all(states.reshape(n, share, STATE), 'sp', 0, 0)]
    all_gather x1, waiting for transfers between devices: 16.1 us -> 22.4 us  [local(): exit_s = lax.all_gather(exit_s, 'sp', axis=1, tiled=True)]
  transfers between devices with their start and end apart: 8 -> 6, of which waited for: 4 -> 3; matrix products, arithmetic and copies ran while one was open for 3% -> 5% of each run, Pallas kernels for 45% -> 62%
where the time goes in v2:
time: 240 us; the launch traced here: 239 us
  Pallas kernels  147 us (61%)
  waiting for transfers between devices  43.5 us (18%)
  between operations  13.4 us (6%)
  local copies, waits for them, and re-layouts  12.7 us (5%)
  matrix products  11.4 us (5%)
  starting transfers between devices  5.69 us (2%)
  other arithmetic  4.67 us (2%)
    pallas_call x1, Pallas kernels, gather_rows(): pl.pallas_call(functools.partial(ring_kernel, n), out_shape=jax.ShapeDtyp...  97.6 us
    all_gather x1, waiting for transfers between devices, local(): exit_s = lax.all_gather(exit_s, 'sp', axis=1, tiled=True)  22.4 us
    pallas_call x1, Pallas kernels, exchange_states(): pl.pallas_call(functools.partial(exchange_kernel, n, share), out_shape=ja...  19.1 us
    ppermute x1, waiting for transfers between devices, local(): arrived = lax.ppermute(away, 'tp', [(0, 1), (1, 0)])  16.5 us
    pallas_call x1, Pallas kernels, project(): pl.pallas_call(project_kernel, grid=(9,), in_specs=[pl.BlockSpec((count,...  15.2 us
    pallas_call x1, Pallas kernels, local(): pl.pallas_call(mix_kernel, grid=(pairs,), in_specs=[pl.BlockSpec((full, c...  10.2 us
    unnamed x37, local copies, waits for them, and re-layouts  7.41 us
    pallas_call x1, Pallas kernels, local(): pl.pallas_call(finish_kernel, grid=(pairs,), in_specs=[pl.BlockSpec((leng...  5.28 us
  transfers between devices with their start and end apart: 6, of which 3 were waited for; matrix products, arithmetic and copies ran while one was open for 5% of the time, Pallas kernels for 62%

profile of v2, /device:TPU:0, one launch (start us, length us, event | category | flops | bytes accessed | tf_op | source)
XLA Modules:
  0.0 238.8 jit_solution(6362669877391688031)
XLA Ops:
  6.5 0.7 convert_element_type.30
  7.3 1.4 fusion.3
  8.6 1.4 fusion.5
  10.1 2.5 %collective-permute-start = (bf16[8,2048]{1,0:T(8,128)(2,1)S(1)}, bf16[8,2048]{1,0:T(8,128)(2,1)S(1)}, u32[]{:S(2)}, u32[]{:S(2)}) collective-permute-start(bf16[8,2048]{1,0:T(8,128)(2,1)S(1)} %get-tuple-element.23), channel_id=1, source_target_pairs={{0,2},{2,4},{4,6},{6,8},{8,10},{10,12},{12,14},{14,16},{16,18},{18... | collective-permute-start | bytes 98312 | tf_op jit(solution)/shard_map/ppermute | solution.py:349
  12.6 1.4 collective-permute-start.1
  14.1 3.9 %collective-permute-done.1 = bf16[8,2048]{1,0:T(8,128)(2,1)S(1)} collective-permute-done((bf16[8,2048]{1,0:T(8,128)(2,1)S(1)}, bf16[8,2048]{1,0:T(8,128)(2,1)S(1)}, u32[]{:S(2)}, u32[]{:S(2)}) %collective-permute-start.1) | collective-permute-done | bytes 32800 | tf_op jit(solution)/shard_map/ppermute | solution.py:350
  18.0 1.0 pad_maximum_fusion.1
  19.2 97.6 %shard_map.136 = bf16[16,128,4608]{2,1,0:T(8,128)(2,1)S(1)} custom-call(bf16[128,4608]{1,0:T(8,128)(2,1)S(1)} %bitcast_dynamic-update-slice_fusion.w_ref), custom_call_target="tpu_custom_call" | custom-call | bytes 150994944 | tf_op jit(solution)/shard_map/pallas_call | solution.py:112
  116.8 6.4 %copy-done.1 = bf16[16,128,4608]{2,1,0:T(8,128)(2,1)} copy-done((bf16[16,128,4608]{2,1,0:T(8,128)(2,1)}, bf16[16,128,4608]{2,1,0:T(8,128)(2,1)S(1)}, u32[]{:S(2)}) %copy-start.1) | copy-done | bytes 18874392
  125.3 0.8 slice_bitcast_fusion.3
  126.1 1.5 slice_bitcast_fusion.1
  129.2 1.2 copy.18
  130.8 15.2 %shard_map.137.og_ref.ig_ref.va_ref.x_ref.b_ref.c_ref.gate_ref = bf16[400,4608]{1,0:T(8,128)(2,1)} custom-call(bf16[400,2048]{1,0:T(8,128)(2,1)} %copy-done.4, bf16[2048,4608]{1,0:T(8,128)(2,1)} %bitcast.61), custom_call_target="tpu_custom_call" | custom-call | flops 7549747200 | bytes 18874368 | tf_op jit(solution)/shard_map/pallas_call | solution.py:276
  146.0 10.2 %shard_map.138 = (bf16[384,512]{1,0:T(8,128)(2,1)}, f32[384,512]{1,0:T(8,128)}, bf16[384,1024]{1,0:T(8,128)(2,1)}, bf16[1024,128]{1,0:T(8,128)(2,1)}) custom-call(bf16[400,4608]{1,0:T(8,128)(2,1)} %shard_map.137.og_ref.ig_ref.va_ref.x_ref.b_ref.c_ref.gate_ref, bf16[400,4608]{1,0:T(8,128)(2,1)} %shard_map.137.og_ref.ig_ref.va_ref.x_ref.b_ref.c_ref.gate_ref, ...), custom_call_target="tpu_custom_call" | custom-call | flops 1207959552 | bytes 16777216 | tf_op jit(solution)/shard_map/pallas_call | solution.py:386
  156.2 0.7 broadcast_in_dim.5.l_ref
  156.9 19.1 %shard_map.139 = bf16[16,64,128]{2,1,0:T(8,128)(2,1)} custom-call(bf16[16,64,128]{2,1,0:T(8,128)(2,1)} %bitcast.70, f32[16,8,128]{2,1,0:T(8,128)} %broadcast_in_dim.5.l_ref), custom_call_target="tpu_custom_call" | custom-call | bytes 33554432 | tf_op jit(solution)/shard_map/pallas_call | solution.py:252
  176.1 5.3 %shard_map.140 = bf16[384,512]{1,0:T(8,128)(2,1)} custom-call(f32[384,512]{1,0:T(8,128)} %get-tuple-element.15.within_ref, bf16[384,1024]{1,0:T(8,128)(2,1)} %get-tuple-element.16.reads_ref, bf16[1024,128]{1,0:T(8,128)(2,1)} %bitcast.66, bf16[400,4608]{1,0:T(8,128)(2,1)} %shard_map.137.og_ref.ig_ref.va_ref.x_ref.b_ref.c_ref.gate_ref, ...), custom_call_target="tpu_custom_call" | custom-call | tf_op jit(solution)/shard_map/pallas_call | solution.py:428
  181.4 3.4 %fusion.9 = f32[192,2048]{1,0:T(8,128)} fusion(bf16[512,2048]{1,0:T(8,128)(2,1)} %all-gather.5.cloned.1.call-done, bf16[384,512]{1,0:T(8,128)(2,1)S(1)} %copy-done.8, s32[]{:T(128)S(6)} %select_n.14), kind=kOutput, calls=%fused_computation.21 | convolution fusion | flops 402653184 | bytes 3866628 | tf_op jit(solution)/shard_map/dot_general | solution.py:445
  184.7 22.4 %all-gather.7.cloned.1.call-done = bf16[512,2048]{1,0:T(8,128)(2,1)} async-done(((bf16[512,128]{1,0:T(8,128)(2,1)}), bf16[512,2048]{1,0:T(8,128)(2,1)}) %all-gather.7.cloned.1.call-update) | async-done | bytes 2097168 | tf_op jit(solution)/shard_map/all_gather | solution.py:378
  207.1 2.6 %fusion.2 = bf16[192,2048]{1,0:T(8,128)(2,1)S(1)} fusion(f32[192,2048]{1,0:T(8,128)} %fusion.9, bf16[512,2048]{1,0:T(8,128)(2,1)} %all-gather.7.cloned.1.call-done, bf16[384,512]{1,0:T(8,128)(2,1)S(1)} %copy-done.5, s32[]{:T(128)S(6)} %select_n.14), kind=kOutput, calls=%fused_computation.4 | convolution fusion | flops 403439616 | bytes 4653060 | tf_op jit(solution)/shard_map/dot_general | solution.py:446
  209.7 1.7 collective-permute-start.2
  211.4 1.7 fusion.14
  213.1 16.5 %collective-permute-done.2 = bf16[192,2048]{1,0:T(8,128)(2,1)} collective-permute-done((bf16[192,2048]{1,0:T(8,128)(2,1)S(1)}, bf16[192,2048]{1,0:T(8,128)(2,1)}, u32[]{:S(2)}, u32[]{:S(2)}) %collective-permute-start.2) | collective-permute-done | bytes 786464 | tf_op jit(solution)/shard_map/ppermute | solution.py:459
  229.6 2.7 %add_convert_fusion = bf16[192,2048]{1,0:T(8,128)(2,1)} fusion(bf16[192,2048]{1,0:T(8,128)(2,1)} %collective-permute-done.2, f32[192,2048]{1,0:T(8,128)S(1)} %fusion.14, bf16[512,2048]{1,0:T(8,128)(2,1)S(1)} %copy-done.2, bf16[384,512]{1,0:T(8,128)(2,1)S(1)} %copy-done.5, s32[]{:T(128)S(6)} %select_n.13), kind=kOutput, calls=%fused_computation.11 | convolution fusion | flops 405012480 | bytes 5439492 | tf_op jit(solution)/shard_map/dot_general | solution.py:446
  (63 shorter events, 4.2 us)
Async XLA Ops:
  6.5 121.1 %copy-start = (bf16[2048,2,8]{0,2,1:T(8,128)(2,1)S(1)}, bf16[2048,2,8]{0,2,1:T(8,128)(2,1)}, u32[]{:S(2)}) copy-start(bf16[2048,2,8]{0,2,1:T(8,128)(2,1)} %param.19) | copy-start | bytes 196612
  6.5 118.7 %all-gather.9.cloned.1.call-start = ((), (), s32[]{:S(2)}) async-start(), calls=%async_computation.2 | async-start | bytes 2555904 | tf_op jit(solution)/shard_map/all_gather | solution.py:351
  10.0 9.0 %copy-start.9 = (bf16[3,128,512]{2,1,0:T(8,128)(2,1)S(1)}, bf16[3,128,512]{2,1,0:T(8,128)(2,1)}, u32[]{:S(2)}) copy-start(bf16[3,128,512]{2,1,0:T(8,128)(2,1)} %param.16) | copy-start | bytes 1179652
  10.1 4.0 %collective-permute-start = (bf16[8,2048]{1,0:T(8,128)(2,1)S(1)}, bf16[8,2048]{1,0:T(8,128)(2,1)S(1)}, u32[]{:S(2)}, u32[]{:S(2)}) collective-permute-start(bf16[8,2048]{1,0:T(8,128)(2,1)S(1)} %get-tuple-element.23), channel_id=1, source_target_pairs={{0,2},{2,4},{4,6},{6,8},{8,10},{10,12},{12,14},{14,16},{16,18},{18... | collective-permute-start | bytes 98312 | tf_op jit(solution)/shard_map/ppermute | solution.py:349
  12.6 6.5 %copy-start.10 = (bf16[2,128,512]{2,1,0:T(8,128)(2,1)S(1)}, bf16[2,128,512]{2,1,0:T(8,128)(2,1)}, u32[]{:S(2)}) copy-start(bf16[2,128,512]{2,1,0:T(8,128)(2,1)} %param.17) | copy-start | bytes 786436
  12.6 6.5 %copy-start.6 = (bf16[2,128,1024]{2,1,0:T(8,128)(2,1)S(1)}, bf16[2,128,1024]{2,1,0:T(8,128)(2,1)}, u32[]{:S(2)}) copy-start(bf16[2,128,1024]{2,1,0:T(8,128)(2,1)} %param.18) | copy-start | bytes 1572868
  12.6 5.4 %collective-permute-start.1 = (bf16[8,2048]{1,0:T(8,128)(2,1)S(1)}, bf16[8,2048]{1,0:T(8,128)(2,1)S(1)}, u32[]{:S(2)}, u32[]{:S(2)}) collective-permute-start(bf16[8,2048]{1,0:T(8,128)(2,1)S(1)} %get-tuple-element.24), channel_id=1, source_target_pairs={{2,0},{4,2},{6,4},{8,6},{10,8},{12,10},{14,12},{16,14},{18,16},{20... | collective-permute-start | bytes 98312 | tf_op jit(solution)/shard_map/ppermute | solution.py:350
  19.0 162.4 %all-gather.5.cloned.1.call-start = ((), (), s32[]{:S(2)}) async-start(), calls=%async_computation | async-start | bytes 2228224 | tf_op jit(solution)/shard_map/all_gather | solution.py:377
  19.2 104.9 %copy-start.11 = (bf16[5,2,1024]{2,1,0:T(2,128)(2,1)S(1)}, bf16[5,2,1024]{2,1,0:T(2,128)(2,1)}, u32[]{:S(2)}) copy-start(bf16[5,2,1024]{2,1,0:T(2,128)(2,1)} %param.22) | copy-start | bytes 61444
  19.2 105.5 %copy-start.14 = (bf16[512]{0:T(512)(128)(2,1)S(1)}, bf16[512]{0:T(512)(128)(2,1)}, u32[]{:S(2)}) copy-start(bf16[512]{0:T(512)(128)(2,1)} %param.25) | copy-start | bytes 3076
  116.8 6.5 %copy-start.1 = (bf16[16,128,4608]{2,1,0:T(8,128)(2,1)}, bf16[16,128,4608]{2,1,0:T(8,128)(2,1)S(1)}, u32[]{:S(2)}) copy-start(bf16[16,128,4608]{2,1,0:T(8,128)(2,1)S(1)} %shard_map.136) | copy-start | bytes 56623108
  123.3 83.8 %all-gather.7.cloned.1.call-start = ((), (), s32[]{:S(2)}) async-start(), calls=%async_computation.1 | async-start | bytes 2228224 | tf_op jit(solution)/shard_map/all_gather | solution.py:378
  127.7 2.7 %copy-start.4 = (bf16[400,2048]{1,0:T(8,128)(2,1)}, bf16[400,2048]{1,0:T(8,128)(2,1)S(1)}, u32[]{:S(2)}) copy-start(bf16[400,2048]{1,0:T(8,128)(2,1)S(1)} %pad_maximum_fusion.r_ref) | copy-start | bytes 4915204
  127.7 0.7 copy-start.12
  127.7 0.8 copy-start.13
  129.2 16.8 %copy-start.7 = (f32[384,4,8]{0,2,1:T(8,128)}, f32[384,4,8]{0,2,1:T(8,128)S(1)}, u32[]{:S(2)}) copy-start(f32[384,4,8]{0,2,1:T(8,128)S(1)} %reshape.46) | copy-start | bytes 147460
  176.1 5.3 %copy-start.8 = (bf16[384,512]{1,0:T(8,128)(2,1)S(1)}, bf16[384,512]{1,0:T(8,128)(2,1)}, u32[]{:S(2)}) copy-start(bf16[384,512]{1,0:T(8,128)(2,1)} %get-tuple-element.13) | copy-start | bytes 1179652
  181.3 25.8 %copy-start.5 = (bf16[384,512]{1,0:T(8,128)(2,1)S(1)}, bf16[384,512]{1,0:T(8,128)(2,1)}, u32[]{:S(2)}) copy-start(bf16[384,512]{1,0:T(8,128)(2,1)} %shard_map.140) | copy-start | bytes 1179652
  184.7 26.7 %copy-start.3 = (bf16[512,2048]{1,0:T(8,128)(2,1)S(1)}, bf16[512,2048]{1,0:T(8,128)(2,1)}, u32[]{:S(2)}) copy-start(bf16[512,2048]{1,0:T(8,128)(2,1)} %all-gather.5.cloned.1.call-done) | copy-start | bytes 6291460
  209.7 19.9 %collective-permute-start.2 = (bf16[192,2048]{1,0:T(8,128)(2,1)S(1)}, bf16[192,2048]{1,0:T(8,128)(2,1)}, u32[]{:S(2)}, u32[]{:S(2)}) collective-permute-start(bf16[192,2048]{1,0:T(8,128)(2,1)S(1)} %fusion.2), channel_id=1, source_target_pairs={{0,1},{1,0},{2,3},{3,2},{4,5},{5,4},{6,7},{7,6},{8,9},{9,8},{10,11... | collective-permute-start | bytes 2359304 | tf_op jit(solution)/shard_map/ppermute | solution.py:459
  211.4 18.2 %copy-start.2 = (bf16[512,2048]{1,0:T(8,128)(2,1)S(1)}, bf16[512,2048]{1,0:T(8,128)(2,1)}, u32[]{:S(2)}) copy-start(bf16[512,2048]{1,0:T(8,128)(2,1)} %all-gather.7.cloned.1.call-done) | copy-start | bytes 6291460
Sparse Core Ops, SparseCore 0:
  19.1 32.0 all-gather.8
  123.4 40.6 all-gather.4
  166.3 40.8 all-gather.6

commit v3 on v2

--- a/solution.py
+++ b/solution.py
@@ -9,7 +9,7 @@
 
 HEAD_DIM = 64
 STATE = 128
-HALO = 8
+HALO = 16
 CHUNKS = 2
 epsilon = 1e-05
 F32 = jnp.float32
@@ -17,117 +17,239 @@
 HIGHEST = lax.Precision.HIGHEST
 
 
-def ring_kernel(n, w_ref, out_ref, own_sem, ring_send, ring_recv, mate_send, mate_recv):
+def entry_kernel(
+    n, tp, w_ref, x_ref, proj_ref, rows_ref, wbuf, rows, acc, own_sem, ring_send, ring_recv,
+    mate_send, mate_recv, row_sem, row_recv, edge_send, edge_recv,
+):
     chips = n // 2
     me = lax.axis_index("sp")
     core, chip = me % 2, me // 2
     odd = chip % 2
     spot = (1 - odd) * (chip // 2) + odd * (chips - 1 - chip // 2)
+    depth, cols = w_ref.shape
+    full = proj_ref.shape[0]
+    own_rows = x_ref.shape[0]
+
+    def chip_at(position):
+        position = (position + 2 * chips) % chips
+        late = position // ((chips + 1) // 2)
+        return (1 - late) * 2 * position + late * (2 * (chips - 1 - position) + 1)
 
     def device(position):
-        position = (position + 2 * chips) % chips
-        half = (chips + 1) // 2
-        late = position // half
-        late_chip = 2 * (chips - 1 - position) + 1
-        return 2 * ((1 - late) * 2 * position + late * late_chip) + core
+        return 2 * chip_at(position) + core
 
     mate = me + 1 - 2 * core
     ways = (device(spot + 1), device(spot - 1))
-    rows = w_ref.shape[0] // (2 * CHUNKS)
+    cut = (cols // 128 + 1) // 2 * 128
+    spans = ((0, cut), (cut, cols - cut))
+    part_rows = depth // CHUNKS
+    mesh_id = pl.DeviceIdType.MESH
 
     barrier = pltpu.get_barrier_semaphore()
     for other in (mate,) + ways:
-        pl.semaphore_signal(
-            barrier, inc=1, device_id={"sp": other}, device_id_type=pl.DeviceIdType.MESH
-        )
-    pl.semaphore_wait(barrier, 3)
-
-    def piece(way, chunk):
-        return pl.ds((way * CHUNKS + chunk) * rows, rows)
+        pl.semaphore_signal(barrier, inc=1, device_id={"sp": other}, device_id_type=mesh_id)
+    greeted = 3
+    if tp == 2:
+        side = lax.axis_index("tp")
+        for there in (
+            {"tp": 1 - side},
+            {"sp": (me + n - 1) % n, "tp": 1},
+            {"sp": (me + 1) % n, "tp": 0},
+        ):
+            pl.semaphore_signal(barrier, inc=1, device_id=there, device_id_type=mesh_id)
+        greeted = 6
+    pl.semaphore_wait(barrier, greeted)
+
+    def view(ref, owner, way, chunk):
+        start, size = spans[way]
+        part = pl.ds(chunk * part_rows, part_rows)
+        if owner is None:
+            return ref.at[part, pl.ds(start, size)]
+        return ref.at[owner, part, pl.ds(start, size)]
+
+    def owner_of(step, way):
+        return device(spot - step if way == 0 else spot + step)
+
+    def send(step, way, chunk, owner, out_sem, in_sem, there):
+        return pltpu.make_async_remote_copy(
+            src_ref=view(w_ref, None, way, chunk) if step == 0 else view(wbuf, owner, way, chunk),
+            dst_ref=view(wbuf, owner, way, chunk),
+            send_sem=out_sem,
+            recv_sem=in_sem,
+            device_id={"sp": there},
+            device_id_type=mesh_id,
+        )
 
     def ring_copy(step, way, chunk):
-        owner = device(spot - step if way == 0 else spot + step)
-        part = piece(way, chunk)
-        return pltpu.make_async_remote_copy(
-            src_ref=w_ref.at[part] if step == 0 else out_ref.at[owner, part],
-            dst_ref=out_ref.at[owner, part],
-            send_sem=ring_send.at[step, way, chunk],
-            recv_sem=ring_recv.at[step, way, chunk],
-            device_id={"sp": ways[way]},
-            device_id_type=pl.DeviceIdType.MESH,
-        )
+        at = (step, way, chunk)
+        owner = owner_of(step, way)
+        return send(*at, owner, ring_send.at[at], ring_recv.at[at], ways[way])
 
     def arrival(step, way, chunk):
-        owner = device(spot - step - 1 if way == 0 else spot + step + 1)
-        part = piece(way, chunk)
-        return pltpu.make_async_remote_copy(
-            src_ref=out_ref.at[owner, part],
-            dst_ref=out_ref.at[owner, part],
-            send_sem=ring_send.at[step, way, chunk],
-            recv_sem=ring_recv.at[step, way, chunk],
-            device_id={"sp": ways[way]},
-            device_id_type=pl.DeviceIdType.MESH,
-        )
+        at = (step, way, chunk)
+        owner = owner_of(step + 1, way)
+        return send(1, way, chunk, owner, ring_send.at[at], ring_recv.at[at], ways[way])
 
     def mate_copy(step, way, chunk, incoming=False):
-        owner = device(spot - step if way == 0 else spot + step)
+        at = (step, way, chunk)
+        owner = owner_of(step, way)
         if incoming:
             owner = owner + 1 - 2 * core
-        part = piece(way, chunk)
-        return pltpu.make_async_remote_copy(
-            src_ref=w_ref.at[part] if step == 0 else out_ref.at[owner, part],
-            dst_ref=out_ref.at[owner, part],
-            send_sem=mate_send.at[step, way, chunk],
-            recv_sem=mate_recv.at[step, way, chunk],
-            device_id={"sp": mate},
-            device_id_type=pl.DeviceIdType.MESH,
-        )
+        return send(*at, owner, mate_send.at[at], mate_recv.at[at], mate)
 
     parts = [(way, chunk) for chunk in range(CHUNKS) for way in range(2)]
     for way, chunk in parts:
         ring_copy(0, way, chunk).start()
     for way, chunk in parts:
         mate_copy(0, way, chunk).start()
-    own = pltpu.make_async_copy(w_ref, out_ref.at[me], own_sem)
+    own = pltpu.make_async_copy(w_ref, wbuf.at[me], own_sem.at[0])
     own.start()
+
+    if tp == 2:
+        place = pl.ds(HALO + pl.multiple_of(side * own_rows, HALO), own_rows)
+        other_place = pl.ds(HALO + pl.multiple_of((1 - side) * own_rows, HALO), own_rows)
+        mine = pltpu.make_async_copy(x_ref, rows.at[place], own_sem.at[1])
+        mine.start()
+
+        def row_copy(where):
+            return pltpu.make_async_remote_copy(
+                src_ref=x_ref,
+                dst_ref=rows.at[where],
+                send_sem=row_sem,
+                recv_sem=row_recv,
+                device_id={"tp": 1 - side},
+                device_id_type=mesh_id,
+            )
+
+        def edge_copy(to, where, slot):
+            return pltpu.make_async_remote_copy(
+                src_ref=x_ref.at[pl.ds(pl.multiple_of(side * (own_rows - HALO), HALO), HALO)],
+                dst_ref=rows.at[pl.ds(where, HALO)],
+                send_sem=edge_send.at[to],
+                recv_sem=edge_recv.at[slot],
+                device_id={"sp": (me + n + 2 * side - 1) % n, "tp": to},
+                device_id_type=mesh_id,
+            )
+
+        edge_at = pl.multiple_of((1 - side) * (full - HALO), HALO)
+        row_copy(place).start()
+        for to in range(2):
+            edge_copy(to, edge_at, side).start()
+
+        def rows_ready():
+            mine.wait()
+            row_copy(other_place).wait_recv()
+            edge_copy(0, 0, 1).wait_recv()
+            edge_copy(0, full - HALO, 0).wait_recv()
+            first = jnp.where(me == 0, 0.0, 1.0).astype(BF16)
+            final = jnp.where(me == n - 1, 0.0, 1.0).astype(BF16)
+            rows[pl.ds(0, HALO), :] = rows[pl.ds(0, HALO), :] * first
+            rows[pl.ds(full - HALO, HALO), :] = rows[pl.ds(full - HALO, HALO), :] * final
+            rows_ref[...] = rows[...]
+    else:
+        mine = pltpu.make_async_copy(x_ref, rows, own_sem.at[1])
+        mine.start()
+
+        def rows_ready():
+            mine.wait()
+            rows_ref[...] = rows[...]
+
+    def multiply(step, way, first):
+        for chunk in range(CHUNKS):
+            mate_copy(step, way, chunk, True).wait_recv()
+        where = chip_at(spot - step if way == 0 else spot + step)
+        start, size = spans[way]
+        tile = next(t for t in (768, 512, 256, 128) if size % t == 0)
+        if tp == 2:
+            inner = pl.ds(pl.multiple_of(where * 2 * depth, 2 * depth), 2 * depth)
+
+        @pl.loop(0, size // tile)
+        def _(i):
+            at = pl.ds(pl.multiple_of(start + i * tile, 128), tile)
+            w = wbuf[pl.ds(2 * where, 2), :, at].reshape(2 * depth, tile)
+            lhs = rows[:, inner] if tp == 2 else rows[where]
+            product = jnp.dot(lhs, w, preferred_element_type=F32)
+            if first:
+                acc[:, at] = product
+            else:
+                acc[:, at] += product
+
+    waiting = []
     for step in range(chips - 1):
         for way, chunk in parts:
             arrival(step, way, chunk).wait_recv()
             if step < chips - 2:
                 ring_copy(step + 1, way, chunk).start()
             mate_copy(step + 1, way, chunk).start()
-    own.wait()
+        if step == 0:
+            own.wait()
+            waiting = [0]
+        else:
+            if step == 1:
+                rows_ready()
+            for done in waiting:
+                for way in range(2):
+                    multiply(done, way, done == 0)
+            waiting = []
+        waiting.append(step + 1)
+    for done in waiting:
+        for way in range(2):
+            multiply(done, way, False)
+
+    tile = next(t for t in (768, 512, 384, 256, 128) if cols % t == 0)
+
+    @pl.loop(0, cols // tile)
+    def _(i):
+        at = pl.ds(pl.multiple_of(i * tile, 128), tile)
+        proj_ref[:, at] = acc[:, at].astype(BF16)
+
     for step in range(chips):
         for way, chunk in parts:
             if step < chips - 1:
                 ring_copy(step, way, chunk).wait_send()
             mate_copy(step, way, chunk).wait_send()
-            mate_copy(step, way, chunk, True).wait_recv()
-
-
-def gather_rows(block):
+    if tp == 2:
+        row_copy(place).wait_send()
+        for to in range(2):
+            edge_copy(to, edge_at, side).wait_send()
+
+
+def enter(block, x, full, tp):
     n = lax.axis_size("sp")
     chips = n // 2
-    rows, cols = block.shape
+    depth, cols = block.shape
+    shape = (full, x.shape[1]) if tp == 2 else x.shape
+    vmem = pl.BlockSpec(memory_space=pltpu.VMEM)
+    dma = pltpu.SemaphoreType.DMA
     return pl.pallas_call(
-        functools.partial(ring_kernel, n),
-        out_shape=jax.ShapeDtypeStruct((n, rows, cols), block.dtype),
-        in_specs=[pl.BlockSpec(memory_space=pltpu.VMEM)],
-        out_specs=pl.BlockSpec(memory_space=pl.ANY),
+        functools.partial(entry_kernel, n, tp),
+        out_shape=[
+            jax.ShapeDtypeStruct((full, cols), BF16),
+            jax.ShapeDtypeStruct(shape, BF16),
+        ],
+        in_specs=[vmem, vmem],
+        out_specs=[vmem, vmem],
         scratch_shapes=[
-            pltpu.SemaphoreType.DMA,
-            pltpu.SemaphoreType.DMA((chips - 1, 2, CHUNKS)),
-            pltpu.SemaphoreType.DMA((chips - 1, 2, CHUNKS)),
-            pltpu.SemaphoreType.DMA((chips, 2, CHUNKS)),
-            pltpu.SemaphoreType.DMA((chips, 2, CHUNKS)),
+            pltpu.VMEM((n, depth, cols), BF16),
+            pltpu.VMEM(shape, BF16),
+            pltpu.VMEM((full, cols), F32),
+            dma((2,)),
+            dma((chips - 1, 2, CHUNKS)),
+            dma((chips - 1, 2, CHUNKS)),
+            dma((chips, 2, CHUNKS)),
+            dma((chips, 2, CHUNKS)),
+            dma,
+            dma,
+            dma((2,)),
+            dma((2,)),
         ],
         compiler_params=pltpu.CompilerParams(
-            collective_id=0, has_side_effects=True, vmem_limit_bytes=16 * 2**20
+            collective_id=0, has_side_effects=True, vmem_limit_bytes=56 * 2**20
         ),
         cost_estimate=pl.CostEstimate(
-            flops=0, bytes_accessed=n * rows * cols * 16, transcendentals=0
+            flops=0, bytes_accessed=n * depth * cols * 16, transcendentals=0
         ),
-    )(block)
+    )(block, x)
 
 
 def taps_of(padded, table, length):
@@ -265,29 +387,6 @@
     )(states, tables)
 
 
-def project_kernel(r_ref, w_ref, o_ref):
-    o_ref[...] = jnp.dot(r_ref[...], w_ref[...], preferred_element_type=F32).astype(BF16)
-
-
-def project(rows, weights):
-    count, width = rows.shape
-    cols = weights.shape[1]
-    tile = cols // 9
-    return pl.pallas_call(
-        project_kernel,
-        grid=(9,),
-        in_specs=[
-            pl.BlockSpec((count, width), lambda j: (0, 0)),
-            pl.BlockSpec((width, tile), lambda j: (0, j)),
-        ],
-        out_specs=pl.BlockSpec((count, tile), lambda j: (0, j)),
-        out_shape=jax.ShapeDtypeStruct((count, cols), BF16),
-        cost_estimate=pl.CostEstimate(
-            flops=2 * count * width * cols, bytes_accessed=2 * width * cols, transcendentals=0
-        ),
-    )(rows, weights)
-
-
 def finish_kernel(within_ref, reads_ref, enter_ref, gate_ref, gain_ref, col_ref, y_ref):
     length = y_ref.shape[0]
     cols = col_ref[0]
@@ -335,8 +434,6 @@
         + [latent_write_read_matrix[i] for i in range(2)],
         axis=1,
     )
-    gathered = gather_rows(block)
-    weights = gathered.reshape(n * block.shape[0], block.shape[1])
 
     x32 = layer_source_rows.astype(F32)
     normed = (
@@ -344,17 +441,17 @@
         * lax.rsqrt(jnp.mean(x32 * x32, axis=-1, keepdims=True) + epsilon)
         * entry_rescale_factor.astype(F32)
     ).astype(BF16)
-    up = [(i, i + 1) for i in range(n - 1)]
-    down = [(i + 1, i) for i in range(n - 1)]
-    before = lax.ppermute(normed[own_rows - HALO :], "sp", up)
-    after = lax.ppermute(normed[:HALO], "sp", down)
-    shared = lax.all_gather(jnp.concatenate([before, normed, after], axis=0), "tp", axis=0)
-    rows = jnp.concatenate(
-        [shared[tp - 1, :HALO]]
-        + [shared[i, HALO : HALO + own_rows] for i in range(tp)]
-        + [shared[0, HALO + own_rows :]],
-        axis=0,
-    )
+    if tp == 2:
+        proj, rows = enter(block, normed, full, tp)
+    else:
+        up = [(i, i + 1) for i in range(n - 1)]
+        down = [(i + 1, i) for i in range(n - 1)]
+        shared = lax.all_gather(normed, "tp", axis=0, tiled=True)
+        before = lax.ppermute(shared[length - HALO :], "sp", up)
+        after = lax.ppermute(shared[:HALO], "sp", down)
+        rows = jnp.concatenate([before, shared, after], axis=0)
+        slabs = rows.reshape(full, n // 2, 2 * block.shape[0]).transpose(1, 0, 2)
+        proj, _ = enter(block, slabs, full, tp)
 
     step_weight = timestep_matrix.reshape(width, 2 * heads)
     raw = jnp.dot(rows, step_weight, preferred_element_type=F32).astype(BF16)
@@ -370,12 +467,9 @@
     span_log = jnp.stack([run_f[length - 1], run_b[0]], axis=1)
     share = heads * 2 * HEAD_DIM // n
 
-    exit_c, exit_s, weights = lax.optimization_barrier(
-        (sliding_mixer_exit_matrix, recurrent_mixer_exit_matrix, weights)
-    )
-    proj = project(rows, weights)
+    exit_c, proj = lax.optimization_barrier((sliding_mixer_exit_matrix, proj))
     exit_c = lax.all_gather(exit_c, "sp", axis=1, tiled=True)
-    exit_s = lax.all_gather(exit_s, "sp", axis=1, tiled=True)
+    exit_s = lax.all_gather(recurrent_mixer_exit_matrix, "sp", axis=1, tiled=True)
 
     latent = latent_kernel_coefficients
     pw, sw = 2 * HEAD_DIM, 2 * STATE

time: 240 us -> 241 us (level)
  waiting for transfers between devices: 43.5 us -> 55.3 us
  starting transfers between devices: 5.69 us -> 1.91 us
  local copies, waits for them, and re-layouts: 12.7 us -> 9.33 us
  other arithmetic: 4.67 us -> 1.51 us
    all_gather x2 -> x1, waiting for transfers between devices: 22.4 us -> 38.2 us  [local(): lax.all_gather(recurrent_mixer_exit_matrix, 'sp', axis=1, tiled=True)]
    pallas_call x2 -> x1, Pallas kernels: 113 us -> 105 us  [enter(): pl.pallas_call(functools.partial(entry_kernel, n, tp), out_shape=[jax.Sha...]
    pallas_call x1, Pallas kernels: 19.1 us -> 24.8 us  [exchange_states(): pl.pallas_call(functools.partial(exchange_kernel, n, share), out_shape=ja...]
    ppermute x2 -> x0, starting transfers between devices: 3.95 us -> none  [the longest x1 2.53 us: local(): before = lax.ppermute(normed[own_rows - HALO:], 'sp', up)]
    ppermute x2 -> x0, waiting for transfers between devices: 3.92 us -> none  [the longest x1 3.91 us: local(): after = lax.ppermute(normed[:HALO], 'sp', down)]
    unnamed x37 -> x35, local copies, waits for them, and re-layouts: 7.41 us -> 6.33 us
  transfers between devices with their start and end apart: 6 -> 3, of which waited for: 3 -> 2; matrix products, arithmetic and copies ran while one was open for 5% -> 5% of each run, Pallas kernels for 62% -> 17%
where the time goes in v3:
time: 241 us; the launch traced here: 240 us
  Pallas kernels  145 us (60%)
  waiting for transfers between devices  55.3 us (23%)
  between operations  13.6 us (6%)
  matrix products  12.9 us (5%)
  local copies, waits for them, and re-layouts  9.33 us (4%)
    pallas_call x1, Pallas kernels, enter(): pl.pallas_call(functools.partial(entry_kernel, n, tp), out_shape=[jax.Sha...  105 us
    all_gather x1, waiting for transfers between devices, local(): lax.all_gather(recurrent_mixer_exit_matrix, 'sp', axis=1, tiled=True)  38.2 us
    pallas_call x1, Pallas kernels, exchange_states(): pl.pallas_call(functools.partial(exchange_kernel, n, share), out_shape=ja...  24.8 us
    ppermute x1, waiting for transfers between devices, local(): arrived = lax.ppermute(away, 'tp', [(0, 1), (1, 0)])  16.5 us
    pallas_call x1, Pallas kernels, local(): pl.pallas_call(mix_kernel, grid=(pairs,), in_specs=[pl.BlockSpec((full, c...  10.3 us
    unnamed x35, local copies, waits for them, and re-layouts  6.33 us
    pallas_call x1, Pallas kernels, local(): pl.pallas_call(finish_kernel, grid=(pairs,), in_specs=[pl.BlockSpec((leng...  5.34 us
    dot_general x2, matrix products, partial(): jnp.dot(y_s, exit_s, preferred_element_type=F32)  5.28 us
  transfers between devices with their start and end apart: 3, of which 2 were waited for; matrix products, arithmetic and copies ran while one was open for 5% of the time, Pallas kernels for 17%

profile of v3, /device:TPU:0, one launch (start us, length us, event | category | flops | bytes accessed | tf_op | source)
XLA Modules:
  0.0 240.1 jit_solution(7219344070208907873)
XLA Ops:
  6.6 1.0 bitcast_dynamic-update-slice_fusion.6
  7.6 0.9 bitcast_dynamic-update-slice_fusion.5
  8.5 0.9 bitcast_dynamic-update-slice_fusion.4
  9.4 0.9 bitcast_dynamic-update-slice_fusion.3
  10.4 0.9 bitcast_dynamic-update-slice_fusion.2
  11.3 1.0 bitcast_dynamic-update-slice_fusion.1
  12.6 1.1 fusion.5.x_ref
  13.7 105.1 %shard_map.136 = (bf16[416,4608]{1,0:T(8,128)(2,1)}, bf16[416,2048]{1,0:T(8,128)(2,1)}) custom-call(bf16[128,4608]{1,0:T(8,128)(2,1)} %copy-done.5, bf16[192,2048]{1,0:T(8,128)(2,1)} %fusion.5.x_ref), custom_call_target="tpu_custom_call" | custom-call | bytes 150994944 | tf_op jit(solution)/shard_map/pallas_call | solution.py:224
  119.1 0.5 all-gather.5.cloned.1.call-update
  119.6 2.0 fusion.16
  122.4 1.2 copy.18
  123.6 0.6 copy.20
  124.7 0.6 reshape.45.gain_ref
  125.3 10.3 %shard_map.137 = (bf16[384,512]{1,0:T(8,128)(2,1)}, f32[384,512]{1,0:T(8,128)}, bf16[384,1024]{1,0:T(8,128)(2,1)}, bf16[1024,128]{1,0:T(8,128)(2,1)}) custom-call(bf16[416,4608]{1,0:T(8,128)(2,1)} %get-tuple-element.14.og_ref.ig_ref.va_ref.x_ref.b_ref.c_ref.gate_ref, bf16[416,4608]{1,0:T(8,128)(2,1)} %get-tuple-element.14.og_ref.ig_ref.va_ref.x_ref.b_ref.c_ref.gate_ref, ...), custom_call_target="tpu_custom_call" | custom-call | flops 1207959552 | bytes 16777216 | tf_op jit(solution)/shard_map/pallas_call | solution.py:480
  135.5 0.7 broadcast_in_dim.5.l_ref
  136.3 24.8 %shard_map.138 = bf16[16,64,128]{2,1,0:T(8,128)(2,1)} custom-call(bf16[16,64,128]{2,1,0:T(8,128)(2,1)} %bitcast.57, f32[16,8,128]{2,1,0:T(8,128)} %broadcast_in_dim.5.l_ref), custom_call_target="tpu_custom_call" | custom-call | bytes 33554432 | tf_op jit(solution)/shard_map/pallas_call | solution.py:374
  161.1 5.3 %shard_map.139 = bf16[384,512]{1,0:T(8,128)(2,1)} custom-call(f32[384,512]{1,0:T(8,128)} %get-tuple-element.18.within_ref, bf16[384,1024]{1,0:T(8,128)(2,1)} %get-tuple-element.19.reads_ref, bf16[1024,128]{1,0:T(8,128)(2,1)} %bitcast.53, bf16[416,4608]{1,0:T(8,128)(2,1)} %get-tuple-element.14.og_ref.ig_ref.va_ref.x_ref.b_ref.c_ref.gate_ref, ...), custom_call_target="tpu_custom_call" | custom-call | tf_op jit(solution)/shard_map/pallas_call | solution.py:522
  166.4 3.4 %fusion.9 = f32[192,2048]{1,0:T(8,128)} fusion(bf16[512,2048]{1,0:T(8,128)(2,1)} %all-gather.3.cloned.1.call-done, bf16[384,512]{1,0:T(8,128)(2,1)S(1)} %copy-done.8, s32[]{:T(128)S(6)} %select_n.14), kind=kOutput, calls=%fused_computation.17 | convolution fusion | flops 402653184 | bytes 3866628 | tf_op jit(solution)/shard_map/dot_general | solution.py:539
  169.8 38.2 %all-gather.5.cloned.1.call-done = bf16[512,2048]{1,0:T(8,128)(2,1)} async-done(((bf16[512,128]{1,0:T(8,128)(2,1)}), bf16[512,2048]{1,0:T(8,128)(2,1)}) %all-gather.5.cloned.1.call-update) | async-done | bytes 2097168 | tf_op jit(solution)/shard_map/all_gather | solution.py:472
  208.1 2.6 %fusion.2 = bf16[192,2048]{1,0:T(8,128)(2,1)S(1)} fusion(f32[192,2048]{1,0:T(8,128)} %fusion.9, bf16[512,2048]{1,0:T(8,128)(2,1)} %all-gather.5.cloned.1.call-done, bf16[384,512]{1,0:T(8,128)(2,1)S(1)} %copy-done.4, s32[]{:T(128)S(6)} %select_n.14), kind=kOutput, calls=%fused_computation.4 | convolution fusion | flops 403439616 | bytes 4653060 | tf_op jit(solution)/shard_map/dot_general | solution.py:540
  210.7 1.7 collective-permute-start
  212.4 1.7 fusion.14
  214.0 16.5 %collective-permute-done = bf16[192,2048]{1,0:T(8,128)(2,1)} collective-permute-done((bf16[192,2048]{1,0:T(8,128)(2,1)S(1)}, bf16[192,2048]{1,0:T(8,128)(2,1)}, u32[]{:S(2)}, u32[]{:S(2)}) %collective-permute-start) | collective-permute-done | bytes 786464 | tf_op jit(solution)/shard_map/ppermute | solution.py:553
  230.6 2.7 %add_convert_fusion = bf16[192,2048]{1,0:T(8,128)(2,1)} fusion(bf16[192,2048]{1,0:T(8,128)(2,1)} %collective-permute-done, f32[192,2048]{1,0:T(8,128)S(1)} %fusion.14, bf16[512,2048]{1,0:T(8,128)(2,1)S(1)} %copy-done.1, bf16[384,512]{1,0:T(8,128)(2,1)S(1)} %copy-done.4, s32[]{:T(128)S(6)} %select_n.13), kind=kOutput, calls=%fused_computation.10 | convolution fusion | flops 405012480 | bytes 5439492 | tf_op jit(solution)/shard_map/dot_general | solution.py:540
  (48 shorter events, 1.8 us)
Async XLA Ops:
  6.5 113.1 %copy-start = (bf16[2048,2,8]{0,2,1:T(8,128)(2,1)S(1)}, bf16[2048,2,8]{0,2,1:T(8,128)(2,1)}, u32[]{:S(2)}) copy-start(bf16[2048,2,8]{0,2,1:T(8,128)(2,1)} %param.19) | copy-start | bytes 196612
  6.5 5.7 %copy-start.6 = (bf16[2,128,1024]{2,1,0:T(8,128)(2,1)S(1)}, bf16[2,128,1024]{2,1,0:T(8,128)(2,1)}, u32[]{:S(2)}) copy-start(bf16[2,128,1024]{2,1,0:T(8,128)(2,1)} %param.18) | copy-start | bytes 1572868
  6.5 5.8 %copy-start.11 = (bf16[2048]{0:T(1024)(128)(2,1)S(1)}, bf16[2048]{0:T(1024)(128)(2,1)}, u32[]{:S(2)}) copy-start(bf16[2048]{0:T(1024)(128)(2,1)} %param.15) | copy-start | bytes 12292
  6.5 5.8 %copy-start.3 = (bf16[192,2048]{1,0:T(8,128)(2,1)S(1)}, bf16[192,2048]{1,0:T(8,128)(2,1)}, u32[]{:S(2)}) copy-start(bf16[192,2048]{1,0:T(8,128)(2,1)} %param.14) | copy-start | bytes 2359300
  6.5 159.9 %all-gather.3.cloned.1.call-start = ((), (), s32[]{:S(2)}) async-start(), calls=%async_computation | async-start | bytes 2228224 | tf_op jit(solution)/shard_map/all_gather | solution.py:471
  12.3 1.4 copy-start.5
  13.7 107.9 %copy-start.10 = (f32[384,8]{0,1:T(8,128)S(1)}, f32[384,8]{0,1:T(8,128)}, u32[]{:S(2)}) copy-start(f32[384,8]{0,1:T(8,128)} %param.24) | copy-start | bytes 36868
  13.7 107.9 %copy-start.12 = (f32[2,8]{1,0:T(2,128)S(1)}, f32[2,8]{1,0:T(2,128)}, u32[]{:S(2)}) copy-start(f32[2,8]{1,0:T(2,128)} %param.23) | copy-start | bytes 196
  118.8 89.2 %all-gather.5.cloned.1.call-start = ((), (), s32[]{:S(2)}) async-start(), calls=%async_computation.1 | async-start | bytes 2228224 | tf_op jit(solution)/shard_map/all_gather | solution.py:472
  119.6 4.0 %copy-start.9 = (bf16[5,2,1024]{2,1,0:T(2,128)(2,1)S(1)}, bf16[5,2,1024]{2,1,0:T(2,128)(2,1)}, u32[]{:S(2)}) copy-start(bf16[5,2,1024]{2,1,0:T(2,128)(2,1)} %param.22) | copy-start | bytes 61444
  119.6 5.1 %copy-start.13 = (bf16[512]{0:T(512)(128)(2,1)S(1)}, bf16[512]{0:T(512)(128)(2,1)}, u32[]{:S(2)}) copy-start(bf16[512]{0:T(512)(128)(2,1)} %param.25) | copy-start | bytes 3076
  122.4 2.9 %copy-start.7 = (f32[384,4,8]{0,2,1:T(8,128)}, f32[384,4,8]{0,2,1:T(8,128)S(1)}, u32[]{:S(2)}) copy-start(f32[384,4,8]{0,2,1:T(8,128)S(1)} %reshape.42) | copy-start | bytes 147460
  161.1 5.4 %copy-start.8 = (bf16[384,512]{1,0:T(8,128)(2,1)S(1)}, bf16[384,512]{1,0:T(8,128)(2,1)}, u32[]{:S(2)}) copy-start(bf16[384,512]{1,0:T(8,128)(2,1)} %get-tuple-element.16) | copy-start | bytes 1179652
  166.4 41.6 %copy-start.4 = (bf16[384,512]{1,0:T(8,128)(2,1)S(1)}, bf16[384,512]{1,0:T(8,128)(2,1)}, u32[]{:S(2)}) copy-start(bf16[384,512]{1,0:T(8,128)(2,1)} %shard_map.139) | copy-start | bytes 1179652
  169.8 42.5 %copy-start.2 = (bf16[512,2048]{1,0:T(8,128)(2,1)S(1)}, bf16[512,2048]{1,0:T(8,128)(2,1)}, u32[]{:S(2)}) copy-start(bf16[512,2048]{1,0:T(8,128)(2,1)} %all-gather.3.cloned.1.call-done) | copy-start | bytes 6291460
  210.7 19.9 %collective-permute-start = (bf16[192,2048]{1,0:T(8,128)(2,1)S(1)}, bf16[192,2048]{1,0:T(8,128)(2,1)}, u32[]{:S(2)}, u32[]{:S(2)}) collective-permute-start(bf16[192,2048]{1,0:T(8,128)(2,1)S(1)} %fusion.2), channel_id=1, source_target_pairs={{0,1},{1,0},{2,3},{3,2},{4,5},{5,4},{6,7},{7,6},{8,9},{9,8},{10,11... | collective-permute-start | bytes 2359304 | tf_op jit(solution)/shard_map/ppermute | solution.py:553
  212.4 18.2 %copy-start.1 = (bf16[512,2048]{1,0:T(8,128)(2,1)S(1)}, bf16[512,2048]{1,0:T(8,128)(2,1)}, u32[]{:S(2)}) copy-start(bf16[512,2048]{1,0:T(8,128)(2,1)} %all-gather.5.cloned.1.call-done) | copy-start | bytes 6291460
Sparse Core Ops, SparseCore 0:
  119.0 46.2 all-gather.2
  167.4 40.5 all-gather.4
